TPU v7x, 32 devices: a whole 2x2x4 slice. The times are simulated.
32 devices in a mesh: sp: 8 (over z, core), tp: 4 (over y, x).
Axes of the slice: x: 2, y: 2, z: 4, core: 2. Of those that a mesh axis runs over, the one named last changes fastest.
Arguments:
- residual: bfloat16 [1024, 2048], P('sp'), may hold values from -45 to 45
- query_a: bfloat16 [1024, 16, 128], P('sp', 'tp'), may hold values from -125 to 125
- keys_a: bfloat16 [1024, 16, 128], P('sp', 'tp'), may hold values from -8 to 8
- values_a: bfloat16 [1024, 16, 128], P('sp', 'tp'), may hold values from -6 to 6
- query_b: bfloat16 [1024, 16, 256], P('sp', 'tp'), may hold values from -125 to 125
- keys_b: bfloat16 [1024, 16, 256], P('sp', 'tp'), may hold values from -8 to 8
- values_b: bfloat16 [1024, 16, 256], P('sp', 'tp'), may hold values from -6 to 6
- lambda_a: float32 [16], P('tp'), may hold values from 0.3 to 0.8
- lambda_b: float32 [16], P('tp'), may hold values from 0.3 to 0.8
- gain_a: float32 [128], replicated, may hold values from 0.1 to 1.9
- gain_b: float32 [256], replicated, may hold values from 0.1 to 1.9
- proj_a: bfloat16 [2048, 2048], P('tp'), may hold values from -0.078125 to 0.078125
- proj_b: bfloat16 [4096, 2048], P('tp'), may hold values from -0.078125 to 0.078125
- norm_gain: float32 [2048], replicated, may hold values from 0.1 to 1.9
- routes: int32 [1024, 2], P('sp'), may hold values from 0 to 7, all different within a row; in each aligned block of 128 rows (0 to 127, 128 to 255, ...) at most 64 rows name the same one
- route_weight: float32 [1024, 2], P('sp'), may hold values from 0.2 to 2
- expert_gate: bfloat16 [8, 2048, 2048], P('sp', None, 'tp'), may hold values from -0.125 to 0.125
- expert_up: bfloat16 [8, 2048, 2048], P('sp', None, 'tp'), may hold values from -0.125 to 0.125
- expert_down: bfloat16 [8, 2048, 2048], P('sp', 'tp'), may hold values from -0.125 to 0.125
Outputs:
- layer_out: bfloat16 [1024, 2048], P('sp', 'tp')
Inputs may be any that keep to these rules, and one draw needn't show every extreme that they name: `routes`: each row names 2 different experts; in each aligned block of 128 rows no expert is named more than 64 times, a bound that some block reaches.
All inputs are finite; a program needn't handle non-finite values.
Results may differ from a plain program's by a relative error of at most 0.013.
Values may be sent and summed in bfloat16 or wider, within the bound.
A program may use at most 64 MiB of HBM per device.

v0:
```python
import jax
import jax.numpy as jnp
from jax import lax
from jax.experimental import pallas as pl
from jax.experimental.pallas import tpu as pltpu
from jax.sharding import PartitionSpec as P

DK_A = 64
DK_B = 128
SEG = 64
TOP = 2


EPS = 1e-06


def block_at(ref, index, split):
    if split == "lead":
        return ref.at[index]
    if split == "cols":
        width = ref.shape[-1] // lax.axis_size("tp")
        return ref.at[:, pl.ds(pl.multiple_of(index * width, width), width)]
    return ref


def exchange(array, out_shape, axis, source_split, target_split, collective_id):
    peers = lax.axis_size(axis)

    def kernel(in_ref, out_ref, send_sem, recv_sem):
        me = lax.axis_index(axis)
        barrier = pltpu.get_barrier_semaphore()
        for step in range(1, peers):
            pl.semaphore_signal(
                barrier,
                inc=1,
                device_id={axis: lax.rem(me + step, peers)},
                device_id_type=pl.DeviceIdType.MESH,
            )
        pl.semaphore_wait(barrier, peers - 1)
        copies = []
        for step in range(1, peers):
            peer = lax.rem(me + step, peers)
            copy = pltpu.make_async_remote_copy(
                src_ref=block_at(in_ref, peer, source_split),
                dst_ref=block_at(out_ref, me, target_split),
                send_sem=send_sem.at[step - 1],
                recv_sem=recv_sem.at[step - 1],
                device_id={axis: peer},
                device_id_type=pl.DeviceIdType.MESH,
            )
            copy.start()
            copies.append(copy)
        block_at(out_ref, me, target_split)[...] = block_at(in_ref, me, source_split)[...]
        for copy in copies:
            copy.wait()

    return pl.pallas_call(
        kernel,
        out_shape=jax.ShapeDtypeStruct(out_shape, array.dtype),
        in_specs=[pl.BlockSpec(memory_space=pltpu.VMEM)],
        out_specs=pl.BlockSpec(memory_space=pltpu.VMEM),
        scratch_shapes=[
            pltpu.SemaphoreType.DMA((peers - 1,)),
            pltpu.SemaphoreType.DMA((peers - 1,)),
        ],
        compiler_params=pltpu.CompilerParams(
            collective_id=collective_id, has_side_effects=True, vmem_limit_bytes=16 * 2**20
        ),
        name=f"exchange_{collective_id}",
    )(array)


def greet_peers():
    barrier = pltpu.get_barrier_semaphore()
    total = 0
    for axis in ("sp", "tp"):
        peers = lax.axis_size(axis)
        me = lax.axis_index(axis)
        for step in range(1, peers):
            pl.semaphore_signal(
                barrier,
                inc=1,
                device_id={axis: lax.rem(me + step, peers)},
                device_id_type=pl.DeviceIdType.MESH,
            )
        total += peers - 1
    pl.semaphore_wait(barrier, total)


def send_to(source, target, send_sem, recv_sem, axis, peer):
    copy = pltpu.make_async_remote_copy(
        src_ref=source,
        dst_ref=target,
        send_sem=send_sem,
        recv_sem=recv_sem,
        device_id={axis: peer},
        device_id_type=pl.DeviceIdType.MESH,
    )
    copy.start()
    return copy


def two_axis_call(kernel, array, out_shape, scratch, collective_id):
    seq, heads = lax.axis_size("sp"), lax.axis_size("tp")
    return pl.pallas_call(
        kernel,
        out_shape=jax.ShapeDtypeStruct(out_shape, array.dtype),
        in_specs=[pl.BlockSpec(memory_space=pltpu.VMEM)],
        out_specs=pl.BlockSpec(memory_space=pltpu.VMEM),
        scratch_shapes=list(scratch)
        + [
            pltpu.SemaphoreType.DMA((seq - 1,)),
            pltpu.SemaphoreType.DMA((seq - 1,)),
            pltpu.SemaphoreType.DMA((seq, heads - 1)),
            pltpu.SemaphoreType.DMA((seq, heads - 1)),
        ],
        compiler_params=pltpu.CompilerParams(
            collective_id=collective_id, has_side_effects=True, vmem_limit_bytes=24 * 2**20
        ),
        name=f"two_axis_{collective_id}",
    )(array)


def dispatch(send_rows, collective_id):
    seq, heads = lax.axis_size("sp"), lax.axis_size("tp")
    _, count, width = send_rows.shape

    def kernel(in_ref, out_ref, landed, seq_send, seq_recv, head_send, head_recv):
        seq_me, head_me = lax.axis_index("sp"), lax.axis_index("tp")
        greet_peers()
        first = []
        for step in range(1, seq):
            peer = lax.rem(seq_me + step, seq)
            first.append(
                send_to(
                    in_ref.at[peer],
                    landed.at[seq_me],
                    seq_send.at[step - 1],
                    seq_recv.at[step - 1],
                    "sp",
                    peer,
                )
            )
        second = []
        for step in range(seq):
            source = lax.rem(seq_me + seq - step, seq)
            if step:
                first[step - 1].wait_recv()
            block = landed.at[source] if step else in_ref.at[source]
            place = out_ref.at[
                pl.ds(pl.multiple_of(source * count, count), count),
                pl.ds(pl.multiple_of(head_me * width, width), width),
            ]
            for hop in range(1, heads):
                second.append(
                    send_to(
                        block,
                        place,
                        head_send.at[step, hop - 1],
                        head_recv.at[step, hop - 1],
                        "tp",
                        lax.rem(head_me + hop, heads),
                    )
                )
            place[...] = block[...]
        for copy in first:
            copy.wait_send()
        for copy in second:
            copy.wait()

    return two_axis_call(
        kernel,
        send_rows,
        (seq * count, heads * width),
        [pltpu.VMEM(send_rows.shape, send_rows.dtype)],
        collective_id,
    )


def sum_and_return(down_part, collective_id):
    seq, heads = lax.axis_size("sp"), lax.axis_size("tp")
    count, width = down_part.shape[0] // seq, down_part.shape[1] // heads

    def kernel(in_ref, out_ref, parts, sums, seq_send, seq_recv, head_send, head_recv):
        seq_me, head_me = lax.axis_index("sp"), lax.axis_index("tp")
        greet_peers()

        def piece(owner, column):
            return in_ref.at[
                pl.ds(pl.multiple_of(owner * count, count), count),
                pl.ds(pl.multiple_of(column * width, width), width),
            ]

        steps = list(range(1, seq)) + [0]
        first = {}
        for step in steps:
            owner = lax.rem(seq_me + step, seq)
            for hop in range(1, heads):
                peer = lax.rem(head_me + hop, heads)
                first[step, hop] = send_to(
                    piece(owner, peer),
                    parts.at[owner, head_me],
                    head_send.at[step, hop - 1],
                    head_recv.at[step, hop - 1],
                    "tp",
                    peer,
                )
        second = []
        for step in steps:
            owner = lax.rem(seq_me + step, seq)
            total = piece(owner, head_me)[...].astype(jnp.float32)
            for hop in range(1, heads):
                first[step, hop].wait_recv()
                giver = lax.rem(head_me + heads - hop, heads)
                total = total + parts[owner, giver].astype(jnp.float32)
            rounded = total.astype(out_ref.dtype)
            if step == 0:
                out_ref[owner] = rounded
            else:
                sums[owner] = rounded
                second.append(
                    send_to(
                        sums.at[owner],
                        out_ref.at[seq_me],
                        seq_send.at[step - 1],
                        seq_recv.at[step - 1],
                        "sp",
                        owner,
                    )
                )
        for step in steps:
            for hop in range(1, heads):
                first[step, hop].wait_send()
        for copy in second:
            copy.wait()

    return two_axis_call(
        kernel,
        down_part,
        (seq, count, width),
        [
            pltpu.VMEM((seq, heads, count, width), down_part.dtype),
            pltpu.VMEM((seq, count, width), down_part.dtype),
        ],
        collective_id,
    )


def attend_local(queries, keys_all, values_all, mixing, head_gain, key_size, offset, block_rows):
    tok_rows = queries.shape[0]
    heads_local = queries.shape[1]
    positions = offset + jnp.arange(tok_rows, dtype=jnp.int32)
    query_seg = positions // SEG
    factor = key_size ** (-0.5)
    needed = (offset + tok_rows + block_rows - 1) // block_rows
    first_query = queries[..., :key_size]
    second_query = queries[..., key_size:]

    def block_scores(start, map_query, block_keys):
        raw_scores = (
            jnp.einsum("qhd,khd->hqk", map_query, block_keys, preferred_element_type=jnp.float32)
            * factor
        )
        key_seg = (start + jnp.arange(block_rows, dtype=jnp.int32)) // SEG
        visible = query_seg[:, None] >= key_seg[None, :]
        return jnp.where(visible[None], raw_scores, -jnp.inf)

    def both_scores(block_index):
        start = block_index * block_rows
        block_keys = lax.dynamic_slice_in_dim(keys_all, start, block_rows, 0)
        first_scores = block_scores(start, first_query, block_keys[..., :key_size])
        second_scores = block_scores(start, second_query, block_keys[..., key_size:])
        return (start, first_scores, second_scores)

    def update(old_max, old_sum, scores):
        new_max = jnp.maximum(old_max, jnp.max(scores, axis=-1, keepdims=True))
        new_sum = old_sum * jnp.exp(old_max - new_max) + jnp.sum(
            jnp.exp(scores - new_max), axis=-1, keepdims=True
        )
        return (new_max, new_sum)

    def statistics(block_index, running):
        first_max, first_sum, second_max, second_sum = running
        start, first_scores, second_scores = both_scores(block_index)
        first_max, first_sum = update(first_max, first_sum, first_scores)
        second_max, second_sum = update(second_max, second_sum, second_scores)
        return (first_max, first_sum, second_max, second_sum)

    start_max = jnp.full((heads_local, tok_rows, 1), -jnp.inf, jnp.float32)
    start_sum = jnp.zeros((heads_local, tok_rows, 1), jnp.float32)
    first_max, first_sum, second_max, second_sum = lax.fori_loop(
        0, needed, statistics, (start_max, start_sum, start_max, start_sum)
    )
    mix_col = mixing[:, None, None]

    def accumulate(block_index, summed_rows):
        start, first_scores, second_scores = both_scores(block_index)
        first_probs = jnp.exp(first_scores - first_max) / first_sum
        second_probs = jnp.exp(second_scores - second_max) / second_sum
        block_weights = (first_probs - mix_col * second_probs).astype(jnp.bfloat16)
        block_values = lax.dynamic_slice_in_dim(values_all, start, block_rows, 0)
        return summed_rows + jnp.einsum(
            "hqk,khe->qhe", block_weights, block_values, preferred_element_type=jnp.float32
        )

    mixed = lax.fori_loop(
        0, needed, accumulate, jnp.zeros((tok_rows, heads_local, values_all.shape[2]), jnp.float32)
    )
    mean_sq = jnp.mean(mixed * mixed, axis=-1, keepdims=True)
    return (mixed * lax.rsqrt(mean_sq + EPS) * head_gain).astype(jnp.bfloat16)


def local(
    residual,
    query_a,
    keys_a,
    values_a,
    query_b,
    keys_b,
    values_b,
    lambda_a,
    lambda_b,
    gain_a,
    gain_b,
    proj_a,
    proj_b,
    norm_gain,
    routes,
    route_weight,
    expert_gate,
    expert_up,
    expert_down,
):
    tok_rows = residual.shape[0]
    model_width = residual.shape[1]
    seq_devices = lax.axis_size("sp")
    head_devices = lax.axis_size("tp")
    head_index = lax.axis_index("tp")
    offset = lax.axis_index("sp") * tok_rows
    every_keys_a, every_values_a, every_keys_b, every_values_b = (
        lax.all_gather(keys_a, "sp", axis=0, tiled=True),
        lax.all_gather(values_a, "sp", axis=0, tiled=True),
        lax.all_gather(keys_b, "sp", axis=0, tiled=True),
        lax.all_gather(values_b, "sp", axis=0, tiled=True),
    )
    block_rows = 512
    heads_a = attend_local(
        query_a, every_keys_a, every_values_a, lambda_a, gain_a, DK_A, offset, block_rows
    )
    heads_b = attend_local(
        query_b, every_keys_b, every_values_b, lambda_b, gain_b, DK_B, offset, block_rows
    )
    partial_branch = jnp.dot(
        heads_a.reshape(tok_rows, -1), proj_a, preferred_element_type=jnp.float32
    )
    partial_branch = partial_branch + jnp.dot(
        heads_b.reshape(tok_rows, -1), proj_b, preferred_element_type=jnp.float32
    )
    columns = model_width // head_devices
    col_start = head_index * columns
    branch_parts = exchange(
        partial_branch.astype(jnp.bfloat16),
        (head_devices, tok_rows, columns),
        "tp",
        "cols",
        "lead",
        0,
    )
    summed_cols = jnp.sum(branch_parts.astype(jnp.float32), axis=0)
    residual_cols = lax.dynamic_slice_in_dim(residual, col_start, columns, 1)
    stream_cols = (
        (residual_cols.astype(jnp.float32) + summed_cols).astype(jnp.bfloat16).astype(jnp.float32)
    )
    own_squares = jnp.broadcast_to(jnp.sum(stream_cols * stream_cols, axis=1)[None], (8, tok_rows))
    squares = jnp.sum(
        exchange(own_squares, (head_devices, 8, tok_rows), "tp", "all", "lead", 1)[:, 0], axis=0
    )
    row_scale = lax.rsqrt(squares / model_width + EPS)
    gain_cols = lax.dynamic_slice_in_dim(norm_gain, col_start, columns, 0)
    normed_cols = (stream_cols * row_scale[:, None] * gain_cols).astype(jnp.bfloat16)
    slot_count = 2 * tok_rows * TOP // seq_devices
    assign = routes.reshape(-1)
    onehot = (assign[:, None] == jnp.arange(seq_devices, dtype=jnp.int32)[None, :]).astype(
        jnp.int32
    )
    earlier = jnp.cumsum(onehot, axis=0) - onehot
    slot_index = jnp.sum(earlier * onehot, axis=1)
    target = assign * slot_count + slot_index
    placed = (
        target[:, None] == jnp.arange(seq_devices * slot_count, dtype=jnp.int32)[None, :]
    ).reshape(tok_rows, TOP, -1)
    select = jnp.sum(placed.astype(jnp.bfloat16), axis=1)
    gates = route_weight / jnp.sum(route_weight, axis=1, keepdims=True)
    combine = jnp.sum(placed.astype(jnp.float32) * gates[:, :, None], axis=1)
    send_rows = jnp.einsum(
        "ts,td->sd", select, normed_cols, preferred_element_type=jnp.float32
    ).astype(jnp.bfloat16)
    send_rows = send_rows.reshape(seq_devices, slot_count, columns)
    flat_rows = dispatch(send_rows, 2)
    gate_val = jnp.dot(flat_rows, expert_gate[0], preferred_element_type=jnp.float32)
    up_val = jnp.dot(flat_rows, expert_up[0], preferred_element_type=jnp.float32)
    hidden = (jax.nn.silu(gate_val) * up_val).astype(jnp.bfloat16)
    down_part = jnp.dot(hidden, expert_down[0], preferred_element_type=jnp.float32)
    returned = sum_and_return(down_part.astype(jnp.bfloat16), 3)
    returned_flat = returned.reshape(seq_devices * slot_count, columns).astype(jnp.float32)
    experts_sum = jnp.dot(combine, returned_flat, precision=lax.Precision.HIGHEST)
    return (stream_cols + experts_sum).astype(jnp.bfloat16)


def solution(mesh):
    placed = (
        P("sp", None),
        P("sp", "tp", None),
        P("sp", "tp", None),
        P("sp", "tp", None),
        P("sp", "tp", None),
        P("sp", "tp", None),
        P("sp", "tp", None),
        P("tp"),
        P("tp"),
        P(),
        P(),
        P("tp", None),
        P("tp", None),
        P(),
        P("sp", None),
        P("sp", None),
        P("sp", None, "tp"),
        P("sp", None, "tp"),
        P("sp", "tp", None),
    )
    return jax.shard_map(
        local, mesh=mesh, in_specs=placed, out_specs=P("sp", "tp"), check_vma=False
    )
```

profile of v0, /device:TPU:25, one launch (start us, length us, event | category | flops | bytes accessed | tf_op | source)
XLA Modules:
  0.0 222.3 jit_solution(12393447433159018626)
XLA Ops:
  7.3 1.7 copy.79
  9.8 1.8 copy.84
  11.6 0.8 copy.89
  12.7 1.1 fusion.126
  16.0 0.8 fusion.114
  16.8 0.8 select_reduce_fusion
  17.7 1.3 dynamic_slice.43
  19.0 12.3 %all-gather.7.cloned.1.call-done = bf16[1024,4,128]{2,1,0:T(4,128)(2,1)} async-done(((bf16[128,4,128]{2,1,0:T(4,128)(2,1)}), bf16[1024,4,128]{2,1,0:T(4,128)(2,1)}) %all-gather.7.cloned.1.call-update) | async-done | bytes 1048592 | tf_op jit(solution)/shard_map/all_gather | solution.py:341
  31.3 1.6 copy.83
  34.2 6.8 %while.64 = (s32[]{:T(128)}, f32[4,128,1]{1,0,2:T(4,128)S(1)}, f32[4,128,1]{1,0,2:T(4,128)}, f32[4,128,1]{1,0,2:T(4,128)S(1)}, f32[4,128,1]{1,0,2:T(4,128)}, /*i...) while((s32[]{:T(128)}, f32[4,128,1]{1,0,2:T(4,128)S(1)}, ...), condition=%wide.region_5.6_spmd.clone, body=%wide.region_0.5_spmd.clone.sunk | while | flops 69808128 | bytes 5104859 | solution.py:291
  34.3 1.2 fusion.170
  36.3 1.3 bitcast_add_fusion.6
  37.7 1.2 fusion.170
  39.7 1.3 bitcast_add_fusion.6
  41.0 15.8 %all-gather.5.cloned.1.call-done = bf16[1024,4,128]{0,2,1:T(8,128)(2,1)} async-done(((bf16[128,4,128]{0,2,1:T(8,128)(2,1)}), bf16[1024,4,128]{0,2,1:T(8,128)(2,1)}) %all-gather.5.cloned.1.call-update) | async-done | bytes 1048592 | tf_op jit(solution)/shard_map/all_gather | solution.py:342
  57.5 12.1 %while.65 = (s32[]{:T(128)}, f32[128,4,128]{0,2,1:T(8,128)}, s32[]{:T(128)}, bf16[1024,4,128]{0,2,1:T(8,128)(2,1)}, bf16[1024,4,128]{0,2,1:T(8,128)(2,1)S(1)}, /...) while((s32[]{:T(128)}, f32[128,4,128]{0,2,1:T(8,128)}, ...), condition=%wide.region_7.8_spmd.clone, body=%wide.region_6.7_spmd.clone.sunk | while | flops 137242624 | bytes 4282679 | solution.py:306
  57.5 0.8 broadcast_compare_fusion.9
  58.3 2.4 %fusion.177 = f32[4,128,512]{1,2,0:T(8,128)} fusion(bf16[128,4,64]{0,2,1:T(8,128)(2,1)S(1)} %get-tuple-element.1403, f32[4,128]{1,0:T(4,128)} %bitcast.241, f32[4,128]{1,0:T(4,128)S(1)} %bitcast.239, f32[4]{0:T(128)} %bitcast.245, pred[128,512]{0,1:T(8,128)(4,1)} %broadcast_compare_fusion.9, bf16[1024,4,128]{0,2,1:T(8,128)(2,1)S(1)} %get-tuple-element.1398, ...), kind=kOutput, calls=%fused_computation.47.clone.1 | convolution fusion | flops 34865152 | bytes 1445912 | tf_op jit(solution)/shard_map/while/body/qhd,khd->hqk/dot_general | solution.py:261
  60.7 2.9 %fusion.178 = f32[128,4,128]{0,2,1:T(8,128)} fusion(f32[128,4,128]{0,2,1:T(8,128)} %get-tuple-element.1377, f32[4,128,512]{1,2,0:T(8,128)} %fusion.177, bf16[128,4,64]{0,2,1:T(8,128)(2,1)S(1)} %copy-done.3, f32[4,128]{1,0:T(4,128)S(1)} %bitcast.240, f32[4,128]{1,0:T(4,128)S(1)} %bitcast.238, bf16[1024,4,128]{0,2,1:T(8,128)(2,1)} %get-tuple-element.1397, ...), kind=kOutput, calls=%fused_computation.51.clone.1 | convolution fusion | flops 102301696 | bytes 2495488 | tf_op jit(solution)/shard_map/while/body/hqk,khe->qhe/dot_general | solution.py:302
  64.4 2.4 %fusion.177 = f32[4,128,512]{1,2,0:T(8,128)} fusion(bf16[128,4,64]{0,2,1:T(8,128)(2,1)S(1)} %get-tuple-element.1403, f32[4,128]{1,0:T(4,128)} %bitcast.241, f32[4,128]{1,0:T(4,128)S(1)} %bitcast.239, f32[4]{0:T(128)} %bitcast.245, pred[128,512]{0,1:T(8,128)(4,1)} %broadcast_compare_fusion.9, bf16[1024,4,128]{0,2,1:T(8,128)(2,1)S(1)} %get-tuple-element.1398, ...), kind=kOutput, calls=%fused_computation.47.clone.1 | convolution fusion | flops 34865152 | bytes 1445912 | tf_op jit(solution)/shard_map/while/body/qhd,khd->hqk/dot_general | solution.py:261
  66.8 2.9 %fusion.178 = f32[128,4,128]{0,2,1:T(8,128)} fusion(f32[128,4,128]{0,2,1:T(8,128)} %get-tuple-element.1377, f32[4,128,512]{1,2,0:T(8,128)} %fusion.177, bf16[128,4,64]{0,2,1:T(8,128)(2,1)S(1)} %copy-done.3, f32[4,128]{1,0:T(4,128)S(1)} %bitcast.240, f32[4,128]{1,0:T(4,128)S(1)} %bitcast.238, bf16[1024,4,128]{0,2,1:T(8,128)(2,1)} %get-tuple-element.1397, ...), kind=kOutput, calls=%fused_computation.51.clone.1 | convolution fusion | flops 102301696 | bytes 2495488 | tf_op jit(solution)/shard_map/while/body/hqk,khe->qhe/dot_general | solution.py:302
  69.6 1.0 multiply_reduce_fusion.1
  70.6 1.0 multiply_convert_fusion.1
  71.7 3.1 %fusion.128 = f32[128,2048]{1,0:T(8,128)} fusion(bf16[128,512]{0,1:T(8,128)(2,1)S(1)} %bitcast.235, bf16[512,2048]{1,0:T(8,128)(2,1)} %param.38), kind=kOutput, calls=%fused_computation.202 | convolution fusion | flops 268435456 | bytes 3276800 | tf_op jit(solution)/shard_map/dot_general | solution.py:353
  74.8 11.0 %all-gather.11.cloned.1.call-done = bf16[1024,4,256]{2,1,0:T(4,128)(2,1)} async-done(((bf16[128,4,256]{2,1,0:T(4,128)(2,1)}), bf16[1024,4,256]{2,1,0:T(4,128)(2,1)}) %all-gather.11.cloned.1.call-update) | async-done | bytes 2097168 | tf_op jit(solution)/shard_map/all_gather | solution.py:343
  85.8 3.2 %copy.88 = bf16[1024,4,256]{2,0,1:T(8,128)(2,1)} copy(bf16[1024,4,256]{2,1,0:T(4,128)(2,1)} %all-gather.11.cloned.1.call-done) | data formatting | bytes 4194304
  89.0 6.7 %while.66 = (s32[]{:T(128)}, f32[4,128,1]{1,0,2:T(4,128)S(1)}, f32[4,128,1]{1,0,2:T(4,128)S(1)}, f32[4,128,1]{1,0,2:T(4,128)S(1)}, f32[4,128,1]{1,0,2:T(4,128)S(...) while((s32[]{:T(128)}, f32[4,128,1]{1,0,2:T(4,128)S(1)}, ...), condition=%wide.region_14.15_spmd.clone, body=%wide.region_9.14_spmd.clone.sunk | while | flops 136916992 | bytes 5760219 | solution.py:291
  89.2 1.4 fusion.181
  90.8 1.4 fusion.182
  92.6 1.4 fusion.181
  94.1 1.4 fusion.182
  95.8 20.8 %all-gather.9.cloned.1.call-done = bf16[1024,4,256]{0,2,1:T(8,128)(2,1)} async-done(((bf16[128,4,256]{0,2,1:T(8,128)(2,1)}), bf16[1024,4,256]{0,2,1:T(8,128)(2,1)}) %all-gather.9.cloned.1.call-update) | async-done | bytes 2097168 | tf_op jit(solution)/shard_map/all_gather | solution.py:344
  116.6 10.5 %while.67 = (s32[]{:T(128)}, f32[128,4,256]{0,2,1:T(8,128)S(1)}, s32[]{:T(128)}, bf16[1024,4,256]{0,2,1:T(8,128)(2,1)}, bf16[1024,4,256]{2,0,1:T(8,128)(2,1)}, /...) while((s32[]{:T(128)}, f32[128,4,256]{0,2,1:T(8,128)S(1)}, ...), condition=%wide.region_16.17_spmd.clone, body=%wide.region_15.16_spmd.clone.sunk | while | flops 271525888 | bytes 5716223 | solution.py:306
  116.8 2.5 %fusion.188 = f32[4,128,512]{1,2,0:T(8,128)} fusion(bf16[128,4,128]{2,0,1:T(8,128)(2,1)S(1)} %get-tuple-element.1502, bf16[1024,4,256]{2,0,1:T(8,128)(2,1)} %get-tuple-element.1497, s32[]{:T(128)S(6)} %select_n.263, s32[]{:T(128)S(6)} %add.731, f32[4,128]{1,0:T(4,128)S(1)} %bitcast.243, f32[4,128]{1,0:T(4,128)S(1)} %bitcast.237, ...), kind=kOutput, calls=%fused_computation.121.clone.1 | convolution fusion | flops 68419584 | bytes 1773592 | tf_op jit(solution)/shard_map/while/body/qhd,khd->hqk/dot_general | solution.py:261
  119.3 2.5 %fusion.189 = f32[128,4,256]{0,2,1:T(8,128)S(1)} fusion(f32[128,4,256]{0,2,1:T(8,128)S(1)} %get-tuple-element.1476, f32[4,128,512]{1,2,0:T(8,128)} %fusion.188, bf16[128,4,128]{2,0,1:T(8,128)(2,1)S(1)} %get-tuple-element.1498, bf16[1024,4,256]{0,2,1:T(8,128)(2,1)} %get-tuple-element.1496, s32[]{:T(128)S(6)} %select_n.263, ...), kind=kOutput, calls=%fused_computation.124.clone.1 | convolution fusion | flops 203030528 | bytes 3871744 | tf_op jit(solution)/shard_map/while/body/hqk,khe->qhe/dot_general | solution.py:302
  122.0 2.5 %fusion.188 = f32[4,128,512]{1,2,0:T(8,128)} fusion(bf16[128,4,128]{2,0,1:T(8,128)(2,1)S(1)} %get-tuple-element.1502, bf16[1024,4,256]{2,0,1:T(8,128)(2,1)} %get-tuple-element.1497, s32[]{:T(128)S(6)} %select_n.263, s32[]{:T(128)S(6)} %add.731, f32[4,128]{1,0:T(4,128)S(1)} %bitcast.243, f32[4,128]{1,0:T(4,128)S(1)} %bitcast.237, ...), kind=kOutput, calls=%fused_computation.121.clone.1 | convolution fusion | flops 68419584 | bytes 1773592 | tf_op jit(solution)/shard_map/while/body/qhd,khd->hqk/dot_general | solution.py:261
  124.5 2.5 %fusion.189 = f32[128,4,256]{0,2,1:T(8,128)S(1)} fusion(f32[128,4,256]{0,2,1:T(8,128)S(1)} %get-tuple-element.1476, f32[4,128,512]{1,2,0:T(8,128)} %fusion.188, bf16[128,4,128]{2,0,1:T(8,128)(2,1)S(1)} %get-tuple-element.1498, bf16[1024,4,256]{0,2,1:T(8,128)(2,1)} %get-tuple-element.1496, s32[]{:T(128)S(6)} %select_n.263, ...), kind=kOutput, calls=%fused_computation.124.clone.1 | convolution fusion | flops 203030528 | bytes 3871744 | tf_op jit(solution)/shard_map/while/body/hqk,khe->qhe/dot_general | solution.py:302
  127.3 3.2 %fusion.94.in_ref = bf16[128,2048]{1,0:T(8,128)(2,1)S(1)} fusion(f32[128,2048]{1,0:T(8,128)} %fusion.128, bf16[128,1024]{0,1:T(8,128)(2,1)S(1)} %bitcast.230, bf16[1024,2048]{1,0:T(8,128)(2,1)} %param.39), kind=kOutput, calls=%fused_computation.153 | convolution fusion | flops 537395200 | bytes 6029312 | tf_op jit(solution)/shard_map/dot_general | solution.py:356
  130.6 9.2 %exchange_0.1 = bf16[4,128,512]{2,1,0:T(8,128)(2,1)S(1)} custom-call(bf16[128,2048]{1,0:T(8,128)(2,1)S(1)} %fusion.94.in_ref), custom_call_target="tpu_custom_call" | custom-call | tf_op jit(solution)/shard_map/exchange_0/pallas_call | solution.py:57
  139.9 1.2 fusion.111
  141.1 3.5 %exchange_1.1 = f32[4,8,128]{2,1,0:T(8,128)S(1)} custom-call(f32[8,128]{1,0:T(8,128)S(1)} %broadcast_in_dim.185.in_ref), custom_call_target="tpu_custom_call" | custom-call | tf_op jit(solution)/shard_map/exchange_1/pallas_call | solution.py:57
  145.0 29.9 %two_axis_2.1 = bf16[512,2048]{1,0:T(8,128)(2,1)S(1)} custom-call(bf16[8,64,512]{2,1,0:T(8,128)(2,1)S(1)} %bitcast.228), custom_call_target="tpu_custom_call" | custom-call | tf_op jit(solution)/shard_map/two_axis_2/pallas_call | solution.py:105
  174.9 1.3 copy-done.1
  176.2 1.2 fusion.98
  177.5 6.0 %convolution_convert_fusion.in_ref = bf16[512,2048]{1,0:T(8,128)(2,1)} fusion(bf16[1,512,2048]{2,1,0:T(8,128)(2,1)S(1)} %copy-done, bf16[512,2048]{1,0:T(8,128)(2,1)} %copy-done.1, bf16[1,2048,512]{2,1,0:T(8,128)(2,1)} %param.44, f32[512,512]{1,0:T(8,128)S(1)} %fusion.98), kind=kOutput, calls=%fused_computation.151 | convolution fusion | flops 2150105088 | bytes 9437184 | tf_op jit(solution)/shard_map/dot_general | solution.py:403
  183.4 1.6 copy-done.2
  185.0 29.7 %two_axis_3.1 = bf16[8,64,512]{2,1,0:T(8,128)(2,1)S(1)} custom-call(bf16[512,2048]{1,0:T(8,128)(2,1)S(1)} %copy-done.2), custom_call_target="tpu_custom_call" | custom-call | tf_op jit(solution)/shard_map/two_axis_3/pallas_call | solution.py:105
  214.8 1.0 fusion.106
  (128 shorter events, 10.6 us)
Async XLA Ops:
  6.5 170.9 %copy-start = (bf16[1,512,2048]{2,1,0:T(8,128)(2,1)S(1)}, bf16[1,512,2048]{2,1,0:T(8,128)(2,1)}, u32[]{:S(2)}) copy-start(bf16[1,512,2048]{2,1,0:T(8,128)(2,1)} %param.45) | copy-start | bytes 6291460
  6.5 9.5 %copy-start.9 = (s32[128,2]{0,1:T(2,128)S(1)}, s32[128,2]{0,1:T(2,128)}, u32[]{:S(2)}) copy-start(s32[128,2]{0,1:T(2,128)} %param.41) | copy-start | bytes 3076
  6.5 7.3 %copy-start.5 = (bf16[128,4,128]{2,1,0:T(4,128)(2,1)S(1)}, bf16[128,4,128]{2,1,0:T(4,128)(2,1)}, u32[]{:S(2)}) copy-start(bf16[128,4,128]{2,1,0:T(4,128)(2,1)} %param.28) | copy-start | bytes 393220
  6.5 10.2 %copy-start.10 = (f32[128,2]{0,1:T(2,128)S(1)}, f32[128,2]{0,1:T(2,128)}, u32[]{:S(2)}) copy-start(f32[128,2]{0,1:T(2,128)} %param.42) | copy-start | bytes 3076
  6.5 24.8 %all-gather.7.cloned.1.call-start = ((), (), s32[]{:S(2)}) async-start(), calls=%async_computation.1 | async-start | bytes 1179648 | tf_op jit(solution)/shard_map/all_gather | solution.py:341
  7.3 49.5 %all-gather.5.cloned.1.call-start = ((), (), s32[]{:S(2)}) async-start(), calls=%async_computation | async-start | bytes 1179648 | tf_op jit(solution)/shard_map/all_gather | solution.py:342
  9.0 76.8 %all-gather.11.cloned.1.call-start = ((), (), s32[]{:S(2)}) async-start(), calls=%async_computation.3 | async-start | bytes 2359296 | tf_op jit(solution)/shard_map/all_gather | solution.py:343
  9.7 106.8 %all-gather.9.cloned.1.call-start = ((), (), s32[]{:S(2)}) async-start(), calls=%async_computation.2 | async-start | bytes 2359296 | tf_op jit(solution)/shard_map/all_gather | solution.py:344
  57.5 13.1 %copy-start.12 = (f32[128]{0:T(128)S(1)}, f32[128]{0:T(128)}, u32[]{:S(2)}) copy-start(f32[128]{0:T(128)} %param.36) | copy-start | bytes 1540
  58.3 2.4 %copy-start.3 = (bf16[128,4,64]{0,2,1:T(8,128)(2,1)S(1)}, bf16[128,4,64]{0,2,1:T(8,128)(2,1)}, u32[]{:S(2)}) copy-start(bf16[128,4,64]{0,2,1:T(8,128)(2,1)} %get-tuple-element.1399) | copy-start | bytes 196612 | tf_op jit(solution)/shard_map/while
  58.3 2.4 %copy-start.7 = (f32[4,128,1]{1,0,2:T(4,128)S(1)}, f32[4,128,1]{1,0,2:T(4,128)}, u32[]{:S(2)}) copy-start(f32[4,128,1]{1,0,2:T(4,128)} %get-tuple-element.1401) | copy-start | bytes 6148 | tf_op jit(solution)/shard_map/while
  64.4 2.4 %copy-start.3 = (bf16[128,4,64]{0,2,1:T(8,128)(2,1)S(1)}, bf16[128,4,64]{0,2,1:T(8,128)(2,1)}, u32[]{:S(2)}) copy-start(bf16[128,4,64]{0,2,1:T(8,128)(2,1)} %get-tuple-element.1399) | copy-start | bytes 196612 | tf_op jit(solution)/shard_map/while
  64.4 2.4 %copy-start.7 = (f32[4,128,1]{1,0,2:T(4,128)S(1)}, f32[4,128,1]{1,0,2:T(4,128)}, u32[]{:S(2)}) copy-start(f32[4,128,1]{1,0,2:T(4,128)} %get-tuple-element.1401) | copy-start | bytes 6148 | tf_op jit(solution)/shard_map/while
  89.0 27.6 %copy-start.14 = (f32[4]{0:T(128)S(1)}, f32[4]{0:T(128)}, u32[]{:S(2)}) copy-start(f32[4]{0:T(128)} %param.35) | copy-start | bytes 52
  116.6 10.6 %copy-start.11 = (f32[256]{0:T(256)S(1)}, f32[256]{0:T(256)}, u32[]{:S(2)}) copy-start(f32[256]{0:T(256)} %param.37) | copy-start | bytes 3076
  130.6 14.0 %copy-start.6 = (bf16[128,512]{1,0:T(8,128)(2,1)S(1)}, bf16[128,512]{1,0:T(8,128)(2,1)}, u32[]{:S(2)}) copy-start(bf16[128,512]{1,0:T(8,128)(2,1)} %fusion.114) | copy-start | bytes 393220
  130.6 14.0 %copy-start.8 = (f32[512]{0:T(512)S(1)}, f32[512]{0:T(512)}, u32[]{:S(2)}) copy-start(f32[512]{0:T(512)} %dynamic_slice.43) | copy-start | bytes 6148
  139.9 36.3 %copy-start.13 = (bf16[1,2048,512]{2,1,0:T(8,128)(2,1)S(1)}, bf16[1,2048,512]{2,1,0:T(8,128)(2,1)}, u32[]{:S(2)}) copy-start(bf16[1,2048,512]{2,1,0:T(8,128)(2,1)} %param.43) | copy-start | bytes 6291460
  174.8 1.4 copy-start.1
  183.4 1.6 copy-start.2
  185.0 29.7 %copy-start.4 = (f32[128,512]{1,0:T(8,128)S(1)}, f32[128,512]{1,0:T(8,128)}, u32[]{:S(2)}) copy-start(f32[128,512]{1,0:T(8,128)} %select_reduce_fusion) | copy-start | bytes 786436
Sparse Core Ops, SparseCore 0:
  8.9 22.3 all-gather.6
  32.9 23.7 all-gather.4
  58.4 27.3 all-gather.10
  87.3 29.2 all-gather.8
where the time goes:
time: 224 us; the launch traced here: 222 us
  Pallas kernels  72.3 us (32%)
  waiting for transfers between devices  61.4 us (27%)
  matrix products  44.1 us (20%)
  local copies, waits for them, and re-layouts  18.2 us (8%)
  between operations  13.5 us (6%)
  other arithmetic  12.3 us (5%)
    pallas_call x2, Pallas kernels, two_axis_call(): pl.pallas_call(kernel, out_shape=jax.ShapeDtypeStruct(out_shape, array.dt...  59.6 us
    all_gather x1, waiting for transfers between devices, local(): lax.all_gather(values_b, 'sp', axis=0, tiled=True)  20.8 us
    dot_general x12, matrix products, block_scores(): jnp.einsum('qhd,khd->hqk', map_query, block_keys, preferred_element_type=...  18.5 us
    all_gather x1, waiting for transfers between devices, local(): lax.all_gather(values_a, 'sp', axis=0, tiled=True)  15.8 us
    unnamed x35, local copies, waits for them, and re-layouts  12.9 us
    pallas_call x2, Pallas kernels, exchange(): pl.pallas_call(kernel, out_shape=jax.ShapeDtypeStruct(out_shape, array.dt...  12.7 us
    all_gather x1, waiting for transfers between devices, local(): lax.all_gather(keys_a, 'sp', axis=0, tiled=True)  12.3 us
    all_gather x1, waiting for transfers between devices, local(): lax.all_gather(keys_b, 'sp', axis=0, tiled=True)  11 us
  transfers between devices with their start and end apart: 4, of which 4 were waited for; matrix products, arithmetic and copies ran while one was open for 22% of the time, Pallas kernels for 0%

commit v1 on v0

--- a/solution.py
+++ b/solution.py
@@ -5,8 +5,6 @@
 from jax.experimental.pallas import tpu as pltpu
 from jax.sharding import PartitionSpec as P
 
-DK_A = 64
-DK_B = 128
 SEG = 64
 TOP = 2
 
@@ -246,68 +244,375 @@
     )
 
 
-def attend_local(queries, keys_all, values_all, mixing, head_gain, key_size, offset, block_rows):
-    tok_rows = queries.shape[0]
-    heads_local = queries.shape[1]
-    positions = offset + jnp.arange(tok_rows, dtype=jnp.int32)
-    query_seg = positions // SEG
-    factor = key_size ** (-0.5)
-    needed = (offset + tok_rows + block_rows - 1) // block_rows
-    first_query = queries[..., :key_size]
-    second_query = queries[..., key_size:]
-
-    def block_scores(start, map_query, block_keys):
-        raw_scores = (
-            jnp.einsum("qhd,khd->hqk", map_query, block_keys, preferred_element_type=jnp.float32)
-            * factor
-        )
-        key_seg = (start + jnp.arange(block_rows, dtype=jnp.int32)) // SEG
-        visible = query_seg[:, None] >= key_seg[None, :]
-        return jnp.where(visible[None], raw_scores, -jnp.inf)
-
-    def both_scores(block_index):
-        start = block_index * block_rows
-        block_keys = lax.dynamic_slice_in_dim(keys_all, start, block_rows, 0)
-        first_scores = block_scores(start, first_query, block_keys[..., :key_size])
-        second_scores = block_scores(start, second_query, block_keys[..., key_size:])
-        return (start, first_scores, second_scores)
-
-    def update(old_max, old_sum, scores):
-        new_max = jnp.maximum(old_max, jnp.max(scores, axis=-1, keepdims=True))
-        new_sum = old_sum * jnp.exp(old_max - new_max) + jnp.sum(
-            jnp.exp(scores - new_max), axis=-1, keepdims=True
-        )
-        return (new_max, new_sum)
-
-    def statistics(block_index, running):
-        first_max, first_sum, second_max, second_sum = running
-        start, first_scores, second_scores = both_scores(block_index)
-        first_max, first_sum = update(first_max, first_sum, first_scores)
-        second_max, second_sum = update(second_max, second_sum, second_scores)
-        return (first_max, first_sum, second_max, second_sum)
-
-    start_max = jnp.full((heads_local, tok_rows, 1), -jnp.inf, jnp.float32)
-    start_sum = jnp.zeros((heads_local, tok_rows, 1), jnp.float32)
-    first_max, first_sum, second_max, second_sum = lax.fori_loop(
-        0, needed, statistics, (start_max, start_sum, start_max, start_sum)
-    )
-    mix_col = mixing[:, None, None]
-
-    def accumulate(block_index, summed_rows):
-        start, first_scores, second_scores = both_scores(block_index)
-        first_probs = jnp.exp(first_scores - first_max) / first_sum
-        second_probs = jnp.exp(second_scores - second_max) / second_sum
-        block_weights = (first_probs - mix_col * second_probs).astype(jnp.bfloat16)
-        block_values = lax.dynamic_slice_in_dim(values_all, start, block_rows, 0)
-        return summed_rows + jnp.einsum(
-            "hqk,khe->qhe", block_weights, block_values, preferred_element_type=jnp.float32
-        )
-
-    mixed = lax.fori_loop(
-        0, needed, accumulate, jnp.zeros((tok_rows, heads_local, values_all.shape[2]), jnp.float32)
-    )
-    mean_sq = jnp.mean(mixed * mixed, axis=-1, keepdims=True)
-    return (mixed * lax.rsqrt(mean_sq + EPS) * head_gain).astype(jnp.bfloat16)
+LOG2E = 1.4426950408889634
+MESH = pl.DeviceIdType.MESH
+F32 = jnp.float32
+BF16 = jnp.bfloat16
+
+
+def dot_nt(left, right):
+    return lax.dot_general(left, right, (((1,), (1,)), ((), ())), preferred_element_type=F32)
+
+
+def remote(source, target, send_sem, recv_sem, axis, peer):
+    return pltpu.make_async_remote_copy(
+        src_ref=source,
+        dst_ref=target,
+        send_sem=send_sem,
+        recv_sem=recv_sem,
+        device_id={axis: peer},
+        device_id_type=MESH,
+    )
+
+
+def greet(axes):
+    barrier = pltpu.get_barrier_semaphore()
+    total = 0
+    for axis in axes:
+        peers = lax.axis_size(axis)
+        me = lax.axis_index(axis)
+        for step in range(1, peers):
+            pl.semaphore_signal(
+                barrier, inc=1, device_id={axis: lax.rem(me + step, peers)}, device_id_type=MESH
+            )
+        total += peers - 1
+    pl.semaphore_wait(barrier, total)
+
+
+def columns_of(stats):
+    repeat = stats.shape[1] // stats.shape[0]
+    return jnp.concatenate([stats] * repeat, axis=0).T
+
+
+def rows_of(columns):
+    rows = columns[0].shape[0]
+    lane = lax.broadcasted_iota(jnp.int32, (rows, rows), 1)
+    tile = jnp.zeros((rows, rows), F32)
+    for at, column in enumerate(columns):
+        tile = jnp.where(lane == at, column, tile)
+    return tile.T[: len(columns)]
+
+
+def attention(query_a, keys_a, values_a, query_b, keys_b, values_b, lambdas, gain_a, gain_b):
+    seq = lax.axis_size("sp")
+    rows, heads, width_a = query_a.shape
+    width_b = query_b.shape[2]
+    value_a, value_b = values_a.shape[2], values_b.shape[2]
+    key_a, key_b = width_a // 2, width_b // 2
+    chips = seq // 2
+    half = chips // 2
+    blocks = 2 * half
+    wide_q = width_a + width_b
+    wide_kv = width_a + value_a + width_b + value_b
+    wide_o = value_a + value_b
+    spans = ((0, width_a), (width_a + value_a, width_a + value_a + width_b))
+    factors = (key_a ** (-0.5) * LOG2E, key_b ** (-0.5) * LOG2E)
+
+    def kernel(
+        lam, qa, ka, va, qb, kb, vb, gain_a, gain_b, out_a, out_b,
+        kv, query, far_query, far_stats, own_stats, keep, part, far_part, total, far_total,
+        chain_s, chain_r, part_s, part_r, query_s, query_r, stats_s, stats_r,
+        back_s, back_r, total_s, total_r,
+    ):
+        me = lax.axis_index("sp")
+        chip, core = me // 2, lax.rem(me, 2)
+        upper = chip >= half
+        place = lax.rem(chip, half)
+        base = chip - place
+        middle = 2 * (half - 1) + core
+        is_middle = chip == half - 1
+        partner = 2 * chip + 1 - core
+        above = jnp.minimum(me + 2, seq - 1 - (1 - core))
+        slot = 2 * place + core
+
+        def chain(y, head):
+            ref = kv.at[2 * y + core, head]
+            return remote(ref, ref, chain_s.at[y, head], chain_r.at[y, head], "sp", above)
+
+        def across(y, head):
+            ref = kv.at[2 * y + core, head]
+            return remote(ref, ref, part_s.at[y, head], part_r.at[y, head], "sp", partner)
+
+        def ask(head):
+            return remote(
+                query.at[head], far_query.at[place, head], query_s.at[head],
+                query_r.at[place, head], "sp", middle,
+            )
+
+        def tell(head):
+            return remote(
+                own_stats.at[head], far_stats.at[place, head], stats_s.at[head],
+                stats_r.at[place, head], "sp", middle,
+            )
+
+        def answer(i, head):
+            return remote(
+                part.at[i, head], far_part.at[head], back_s.at[i, head], back_r.at[head],
+                "sp", 2 * (half + i) + core,
+            )
+
+        def answer_total(i, head):
+            return remote(
+                total.at[i, head], far_total.at[head], total_s.at[i, head], total_r.at[head],
+                "sp", 2 * (half + i) + core,
+            )
+
+        def asked(i, head):
+            return remote(
+                query.at[head], far_query.at[i, head], query_s.at[head],
+                query_r.at[i, head], "sp", middle,
+            )
+
+        def told(i, head):
+            return remote(
+                own_stats.at[head], far_stats.at[i, head], stats_s.at[head],
+                stats_r.at[i, head], "sp", middle,
+            )
+
+        greet(("sp",))
+
+        def pack(head):
+            query[head, :, :width_a] = qa[:, head, :]
+            query[head, :, width_a:] = qb[:, head, :]
+            kv[slot, head, :, :width_a] = ka[:, head, :]
+            kv[slot, head, :, spans[0][1] : spans[1][0]] = va[:, head, :]
+            kv[slot, head, :, spans[1][0] : spans[1][1]] = kb[:, head, :]
+            kv[slot, head, :, spans[1][1] :] = vb[:, head, :]
+
+        for head in range(heads):
+            pack(head)
+
+            @pl.when(upper)
+            def _():
+                ask(head).start()
+
+            @pl.when(place < half - 1)
+            def _():
+                chain(place, head).start()
+
+            across(place, head).start()
+
+        def gather(here, head):
+            for y in range(here):
+                chain(y, head).wait_recv()
+                across(y, head).start()
+                if here < half - 1:
+                    chain(y, head).start()
+            for y in range(here + 1):
+                across(y, head).wait_recv()
+
+        def score_maps(ref, head, count):
+            maps = []
+            for group, (width, span) in enumerate(((width_a, spans[0][0]), (width_b, spans[1][0]))):
+                begin = 0 if group == 0 else width_a
+                wide = ref[:, begin : begin + width]
+                block_keys = kv[:count, head, :, span : span + width].reshape(count * rows, width)
+                size = width // 2
+                if size % 128:
+                    lane = lax.broadcasted_iota(jnp.int32, wide.shape, 1)
+                    nothing = jnp.zeros_like(wide)
+                    first = dot_nt(jnp.where(lane < size, wide, nothing), block_keys)
+                    second = dot_nt(jnp.where(lane < size, nothing, wide), block_keys)
+                else:
+                    first = dot_nt(wide[:, :size], block_keys[:, :size])
+                    second = dot_nt(wide[:, size:], block_keys[:, size:])
+                maps += [first * factors[group], second * factors[group]]
+            return maps
+
+        def visible(count):
+            query_seg = (
+                slot * rows + lax.broadcasted_iota(jnp.int32, (rows, 1), 0)
+            ) // SEG
+            key_seg = lax.broadcasted_iota(jnp.int32, (1, count * rows), 1) // SEG
+            return query_seg >= key_seg
+
+        def combine(first, second, head, count, group):
+            weights = (first - second).astype(BF16)
+            begin = spans[group][1]
+            size = value_a if group == 0 else value_b
+            block_values = kv[:count, head, :, begin : begin + size].reshape(count * rows, size)
+            return jnp.dot(weights, block_values, preferred_element_type=F32)
+
+        def finish(mixed, gain, out, head, size):
+            mean_sq = jnp.mean(mixed * mixed, axis=1, keepdims=True)
+            value = (mixed * lax.rsqrt(mean_sq + EPS) * gain[...]).astype(BF16)
+            out[:, pl.ds(pl.multiple_of(head * size, size), size)] = value
+
+        def finish_both(mixed, head):
+            finish(mixed[0], gain_a, out_a, head, value_a)
+            finish(mixed[1], gain_b, out_b, head, value_b)
+
+        def own_lower(head, count):
+            seen = visible(count)
+            maps = [jnp.where(seen, one, -jnp.inf) for one in score_maps(query.at[head], head, count)]
+            mixed = []
+            for group in range(2):
+                parts = []
+                for at in range(2):
+                    scores = maps[2 * group + at]
+                    expo = jnp.exp2(scores - jnp.max(scores, axis=1, keepdims=True))
+                    scale = 1.0 / jnp.sum(expo, axis=1, keepdims=True)
+                    if at:
+                        scale = scale * lam[group, head]
+                    parts.append(expo * scale)
+                mixed.append(combine(parts[0], parts[1], head, count, group))
+            finish_both(mixed, head)
+
+        def for_upper(i, head):
+            asked(i, head).wait_recv()
+            maps = score_maps(far_query.at[i, head], head, blocks)
+            told(i, head).wait_recv()
+            far = columns_of(far_stats[i, head])
+            stats = []
+            for group in range(2):
+                parts = []
+                for at in range(2):
+                    k = 2 * group + at
+                    scores = maps[k]
+                    far_max, far_sum = far[:, k : k + 1], far[:, 4 + k : 5 + k]
+                    top = jnp.maximum(jnp.max(scores, axis=1, keepdims=True), far_max)
+                    expo = jnp.exp2(scores - top)
+                    summed = jnp.sum(expo, axis=1, keepdims=True) + far_sum * jnp.exp2(far_max - top)
+                    stats.append((top, summed))
+                    scale = 1.0 / summed
+                    if at:
+                        scale = scale * lam[group, head]
+                    parts.append(expo * scale)
+                mixed = combine(parts[0], parts[1], head, blocks, group)
+                begin = 0 if group == 0 else value_a
+                part[i, head, :, begin : begin + mixed.shape[1]] = mixed.astype(BF16)
+            answer(i, head).start()
+            total[i, head] = rows_of([one[0] for one in stats] + [one[1] for one in stats])
+            answer_total(i, head).start()
+
+        def upper_first(head, count):
+            seen = visible(count)
+            maps = [jnp.where(seen, one, -jnp.inf) for one in score_maps(query.at[head], head, count)]
+            tops, sums = [], []
+            for k in range(4):
+                top = jnp.max(maps[k], axis=1, keepdims=True)
+                expo = jnp.exp2(maps[k] - top)
+                keep[head, k, :, : count * rows] = expo
+                tops.append(top)
+                sums.append(jnp.sum(expo, axis=1, keepdims=True))
+            own_stats[head] = rows_of(tops + sums)
+            tell(head).start()
+
+        def upper_second(head, count):
+            answer_total(0, head).wait_recv()
+            own = columns_of(own_stats[head])
+            whole = columns_of(far_total[head])
+            scales = []
+            for k in range(4):
+                scale = jnp.exp2(own[:, k : k + 1] - whole[:, k : k + 1]) / whole[:, 4 + k : 5 + k]
+                if k % 2:
+                    scale = scale * lam[k // 2, head]
+                scales.append(scale)
+            mixed = []
+            for group in range(2):
+                first = keep[head, 2 * group, :, : count * rows] * scales[2 * group]
+                second = keep[head, 2 * group + 1, :, : count * rows] * scales[2 * group + 1]
+                mixed.append(combine(first, second, head, count, group))
+            answer(0, head).wait_recv()
+            far = far_part[head].astype(F32)
+            finish_both([mixed[0] + far[:, :value_a], mixed[1] + far[:, value_a:]], head)
+
+        for here in range(half):
+
+            @pl.when((place == here) & jnp.logical_not(upper))
+            def _():
+                def step(head, carry):
+                    gather(here, head)
+                    own_lower(head, 2 * here + 2)
+                    if here == half - 1:
+
+                        def each(i, inner):
+                            for_upper(i, head)
+                            return inner
+
+                        lax.fori_loop(0, half, each, 0)
+                    return carry
+
+                lax.fori_loop(0, heads, step, 0)
+
+            @pl.when((place == here) & upper)
+            def _():
+                def step(head, carry):
+                    gather(here, head)
+                    upper_first(head, 2 * here + 2)
+                    return carry
+
+                lax.fori_loop(0, heads, step, 0)
+
+                def second(head, carry):
+                    upper_second(head, 2 * here + 2)
+                    return carry
+
+                lax.fori_loop(0, heads, second, 0)
+
+            @pl.when(place == here)
+            def _():
+                def drain(head, carry):
+                    for y in range(here + 1):
+                        across(y, head).wait_send()
+                        if here < half - 1:
+                            chain(y, head).wait_send()
+                    return carry
+
+                lax.fori_loop(0, heads, drain, 0)
+
+        @pl.when(upper)
+        def _():
+            def drain(head, carry):
+                ask(head).wait_send()
+                tell(head).wait_send()
+                return carry
+
+            lax.fori_loop(0, heads, drain, 0)
+
+        @pl.when(is_middle)
+        def _():
+            def drain(head, carry):
+                for i in range(half):
+                    answer(i, head).wait_send()
+                    answer_total(i, head).wait_send()
+                return carry
+
+            lax.fori_loop(0, heads, drain, 0)
+
+    vmem = pl.BlockSpec(memory_space=pltpu.VMEM)
+    dma = pltpu.SemaphoreType.DMA
+    return pl.pallas_call(
+        kernel,
+        out_shape=(
+            jax.ShapeDtypeStruct((rows, heads * value_a), BF16),
+            jax.ShapeDtypeStruct((rows, heads * value_b), BF16),
+        ),
+        in_specs=[pl.BlockSpec(memory_space=pltpu.SMEM)] + [vmem] * 8,
+        out_specs=(vmem, vmem),
+        scratch_shapes=[
+            pltpu.VMEM((blocks, heads, rows, wide_kv), BF16),
+            pltpu.VMEM((heads, rows, wide_q), BF16),
+            pltpu.VMEM((half, heads, rows, wide_q), BF16),
+            pltpu.VMEM((half, heads, 8, rows), F32),
+            pltpu.VMEM((heads, 8, rows), F32),
+            pltpu.VMEM((heads, 4, rows, blocks * rows), F32),
+            pltpu.VMEM((half, heads, rows, wide_o), BF16),
+            pltpu.VMEM((heads, rows, wide_o), BF16),
+            pltpu.VMEM((half, heads, 8, rows), F32),
+            pltpu.VMEM((heads, 8, rows), F32),
+            dma((half, heads)), dma((half, heads)), dma((half, heads)), dma((half, heads)),
+            dma((heads,)), dma((half, heads)), dma((heads,)), dma((half, heads)),
+            dma((half, heads)), dma((heads,)), dma((half, heads)), dma((heads,)),
+        ],
+        compiler_params=pltpu.CompilerParams(
+            collective_id=4, has_side_effects=True, vmem_limit_bytes=40 * 2**20
+        ),
+        name="attention",
+    )(
+        lambdas, query_a, keys_a, values_a, query_b, keys_b, values_b,
+        gain_a.reshape(1, -1), gain_b.reshape(1, -1),
+    )
 
 
 def local(
@@ -336,25 +641,22 @@
     seq_devices = lax.axis_size("sp")
     head_devices = lax.axis_size("tp")
     head_index = lax.axis_index("tp")
-    offset = lax.axis_index("sp") * tok_rows
-    every_keys_a, every_values_a, every_keys_b, every_values_b = (
-        lax.all_gather(keys_a, "sp", axis=0, tiled=True),
-        lax.all_gather(values_a, "sp", axis=0, tiled=True),
-        lax.all_gather(keys_b, "sp", axis=0, tiled=True),
-        lax.all_gather(values_b, "sp", axis=0, tiled=True),
-    )
-    block_rows = 512
-    heads_a = attend_local(
-        query_a, every_keys_a, every_values_a, lambda_a, gain_a, DK_A, offset, block_rows
-    )
-    heads_b = attend_local(
-        query_b, every_keys_b, every_values_b, lambda_b, gain_b, DK_B, offset, block_rows
+    heads_a, heads_b = attention(
+        query_a,
+        keys_a,
+        values_a,
+        query_b,
+        keys_b,
+        values_b,
+        jnp.stack([lambda_a, lambda_b]),
+        gain_a,
+        gain_b,
     )
     partial_branch = jnp.dot(
-        heads_a.reshape(tok_rows, -1), proj_a, preferred_element_type=jnp.float32
+        heads_a, proj_a, preferred_element_type=jnp.float32
     )
     partial_branch = partial_branch + jnp.dot(
-        heads_b.reshape(tok_rows, -1), proj_b, preferred_element_type=jnp.float32
+        heads_b, proj_b, preferred_element_type=jnp.float32
     )
     columns = model_width // head_devices
     col_start = head_index * columns

time: 224 us -> 149 us (0.67)
  waiting for transfers between devices: 61.4 us -> 0 us
  Pallas kernels: 72.3 us -> 121 us
  matrix products: 44.1 us -> 11.4 us
  between operations: 13.5 us -> 0.17 us
  other arithmetic: 12.3 us -> 3 us
  local copies, waits for them, and re-layouts: 18.2 us -> 11.4 us
    all_gather x4 -> x0, waiting for transfers between devices: 60 us -> none  [the longest x1 20.8 us: local(): lax.all_gather(values_b, 'sp', axis=0, tiled=True)]
    pallas_call x0 -> x1, Pallas kernels: none -> 48.8 us  [attention(): pl.pallas_call(kernel, out_shape=(jax.ShapeDtypeStruct((rows, heads * val...]
    dot_general x18 -> x2, matrix products: 35.5 us -> 2.83 us  [the longest x1 2.06 us: local(): jnp.dot(heads_a, proj_a, preferred_element_type=jnp.float32)]
    unnamed x35 -> x31, local copies, waits for them, and re-layouts: 12.9 us -> 9.96 us
    add x4 -> x0, other arithmetic: 2.63 us -> none  [update(): old_sum * jnp.exp(old_max - new_max)]
    reduce_sum x10 -> x0, other arithmetic: 2.33 us -> none  [the longest x8 1.3 us: update(): jnp.sum(jnp.exp(scores - new_max), axis=-1, keepdims=True)]
    ge x8 -> x0, other arithmetic: 2.32 us -> none  [block_scores(): visible = query_seg[:, None] >= key_seg[None, :]]
  transfers between devices with their start and end apart: 4 -> 0, of which waited for: 4 -> 0; matrix products, arithmetic and copies ran while one was open for 22% -> 0% of each run, Pallas kernels for 0% -> 0%
where the time goes in v1:
time: 149 us; the launch traced here: 147 us
  Pallas kernels  121 us (81%)
  local copies, waits for them, and re-layouts  11.4 us (8%)
  matrix products  11.4 us (8%)
  other arithmetic  3 us (2%)
    pallas_call x2, Pallas kernels, two_axis_call(): pl.pallas_call(kernel, out_shape=jax.ShapeDtypeStruct(out_shape, array.dt...  59.3 us
    pallas_call x1, Pallas kernels, attention(): pl.pallas_call(kernel, out_shape=(jax.ShapeDtypeStruct((rows, heads * val...  48.8 us
    pallas_call x2, Pallas kernels, exchange(): pl.pallas_call(kernel, out_shape=jax.ShapeDtypeStruct(out_shape, array.dt...  12.8 us
    unnamed x31, local copies, waits for them, and re-layouts  9.96 us
    dot_general x1, matrix products, local(): jnp.dot(hidden, expert_down[0], preferred_element_type=jnp.float32)  5.96 us

profile of v1, /device:TPU:25, one launch (start us, length us, event | category | flops | bytes accessed | tf_op | source)
XLA Modules:
  0.0 147.0 jit_solution(17554209763097282487)
XLA Ops:
  0.0 0.0 copy-start
  0.0 0.8 pad_maximum_fusion.lam
  0.8 0.0 copy-start.3
  0.8 0.9 copy-done.3
  1.8 0.0 copy-start.4
  1.8 0.9 copy-done.4
  2.7 0.0 copy-start.5
  2.7 0.9 copy-done.5
  3.7 0.9 copy-done.6
  4.6 0.0 copy-start.7
  4.6 0.9 copy-done.7
  5.5 0.0 copy-start.8
  5.5 0.9 copy-done.8
  6.4 0.7 copy-done.9
  7.1 0.7 copy-done.10
  7.7 48.8 %attention.1 = (bf16[128,512]{1,0:T(8,128)(2,1)S(1)}, bf16[128,1024]{1,0:T(8,128)(2,1)S(1)}) custom-call(f32[2,4]{1,0:T(2,128)S(1)} %pad_maximum_fusion.lam, bf16[128,4,128]{2,1,0:T(4,128)(2,1)S(1)} %copy-done.6, bf16[128,4,128]{2,1,0:T(4,128)(2,1)S(1)} %copy-done.7, bf16[128,4,128]{2,1,0:T(4,128)(2,1)S(1)} %copy-done.8, bf16[128,4,256]{2,1,0:T(4,128)(2,1)S(1)} %copy-done.3, ...), custom_call_target="tpu_custom_call" | custom-call | tf_op jit(solution)/shard_map/attention/pallas_call | solution.py:585
  56.5 2.1 %fusion.28 = f32[128,2048]{1,0:T(8,128)S(1)} fusion(bf16[128,512]{1,0:T(8,128)(2,1)S(1)} %get-tuple-element.7, bf16[512,2048]{1,0:T(8,128)(2,1)} %param.30), kind=kOutput, calls=%fused_computation.40 | convolution fusion | flops 268435456 | bytes 3276800 | tf_op jit(solution)/shard_map/dot_general | solution.py:655
  58.6 0.0 copy-done.11
  58.6 0.8 fusion.in_ref
  59.4 0.0 copy-start.12
  59.4 9.3 %exchange_0.1 = bf16[4,128,512]{2,1,0:T(8,128)(2,1)S(1)} custom-call(bf16[128,2048]{1,0:T(8,128)(2,1)S(1)} %fusion.in_ref), custom_call_target="tpu_custom_call" | custom-call | tf_op jit(solution)/shard_map/exchange_0/pallas_call | solution.py:55
  68.7 0.1 convert_reduce_fusion
  68.8 1.0 fusion.17
  69.8 3.5 %exchange_1.1 = f32[4,8,128]{2,1,0:T(8,128)S(1)} custom-call(f32[8,128]{1,0:T(8,128)S(1)} %broadcast_in_dim.2.in_ref), custom_call_target="tpu_custom_call" | custom-call | tf_op jit(solution)/shard_map/exchange_1/pallas_call | solution.py:55
  73.4 0.8 dynamic_slice.7
  74.1 0.0 copy-done.12
  74.1 0.1 copy.32
  74.3 0.1 eq.43
  74.4 0.6 reduce-window.6
  75.0 0.2 slice_reduce_fusion
  75.2 0.1 eq.39
  75.4 0.1 fusion.25
  75.5 0.1 reduce_sum.70
  75.6 0.1 copy.34
  75.7 0.1 fusion.20
  75.9 0.4 convolution_convert_fusion.1
  76.2 29.4 %two_axis_2.1 = bf16[512,2048]{1,0:T(8,128)(2,1)S(1)} custom-call(bf16[8,64,512]{2,1,0:T(8,128)(2,1)S(1)} %bitcast.39), custom_call_target="tpu_custom_call" | custom-call | tf_op jit(solution)/shard_map/two_axis_2/pallas_call | solution.py:103
  105.6 0.0 copy-start.1
  105.6 1.3 copy-done.1
  106.9 0.0 copy-done.14
  106.9 1.2 fusion.4
  108.2 0.0 copy-done
  108.2 6.0 %convolution_convert_fusion.in_ref = bf16[512,2048]{1,0:T(8,128)(2,1)} fusion(bf16[1,512,2048]{2,1,0:T(8,128)(2,1)S(1)} %copy-done, bf16[512,2048]{1,0:T(8,128)(2,1)} %copy-done.1, bf16[1,2048,512]{2,1,0:T(8,128)(2,1)} %param.36, f32[512,512]{1,0:T(8,128)S(1)} %fusion.4), kind=kOutput, calls=%fused_computation | convolution fusion | flops 2150105088 | bytes 9437184 | tf_op jit(solution)/shard_map/dot_general | solution.py:705
  114.2 1.6 %copy-done.2 = bf16[512,2048]{1,0:T(8,128)(2,1)S(1)} copy-done((bf16[512,2048]{1,0:T(8,128)(2,1)S(1)}, bf16[512,2048]{1,0:T(8,128)(2,1)}, u32[]{:S(2)}) %copy-start.2) | copy-done | bytes 2097176
  115.7 30.0 %two_axis_3.1 = bf16[8,64,512]{2,1,0:T(8,128)(2,1)S(1)} custom-call(bf16[512,2048]{1,0:T(8,128)(2,1)S(1)} %copy-done.2), custom_call_target="tpu_custom_call" | custom-call | tf_op jit(solution)/shard_map/two_axis_3/pallas_call | solution.py:103
  145.7 0.0 copy-done.13
  145.8 0.1 select_reduce_fusion
  145.9 1.0 fusion.12
  (16 shorter events, 0.1 us)
Async XLA Ops:
  0.0 108.2 %copy-start = (bf16[1,512,2048]{2,1,0:T(8,128)(2,1)S(1)}, bf16[1,512,2048]{2,1,0:T(8,128)(2,1)}, u32[]{:S(2)}) copy-start(bf16[1,512,2048]{2,1,0:T(8,128)(2,1)} %param.37) | copy-start | bytes 6291460
  0.8 0.9 copy-start.3
  1.8 0.9 copy-start.4
  2.7 0.9 copy-start.5
  3.7 0.9 copy-start.6
  4.6 0.9 copy-start.7
  5.5 0.9 copy-start.8
  6.4 0.7 copy-start.9
  7.1 0.7 copy-start.10
  7.7 50.9 %copy-start.11 = (bf16[1024,2048]{1,0:T(8,128)(2,1)S(1)}, bf16[1024,2048]{1,0:T(8,128)(2,1)}, u32[]{:S(2)}) copy-start(bf16[1024,2048]{1,0:T(8,128)(2,1)} %param.31) | copy-start | bytes 12582916
  59.4 14.7 %copy-start.12 = (s32[128,2]{0,1:T(2,128)S(1)}, s32[128,2]{0,1:T(2,128)}, u32[]{:S(2)}) copy-start(s32[128,2]{0,1:T(2,128)} %param.33) | copy-start | bytes 3076
  75.7 31.2 %copy-start.14 = (bf16[1,2048,512]{2,1,0:T(8,128)(2,1)S(1)}, bf16[1,2048,512]{2,1,0:T(8,128)(2,1)}, u32[]{:S(2)}) copy-start(bf16[1,2048,512]{2,1,0:T(8,128)(2,1)} %param.35) | copy-start | bytes 6291460
  105.6 1.4 copy-start.1
  114.2 1.6 %copy-start.2 = (bf16[512,2048]{1,0:T(8,128)(2,1)S(1)}, bf16[512,2048]{1,0:T(8,128)(2,1)}, u32[]{:S(2)}) copy-start(bf16[512,2048]{1,0:T(8,128)(2,1)} %convolution_convert_fusion.in_ref) | copy-start | bytes 6291460
  115.7 30.0 %copy-start.13 = (f32[128,2]{0,1:T(2,128)S(1)}, f32[128,2]{0,1:T(2,128)}, u32[]{:S(2)}) copy-start(f32[128,2]{0,1:T(2,128)} %param.34) | copy-start | bytes 3076

commit v2 on v0

v2 whole, which is shorter than its diff:
```python
import math

import jax
import jax.numpy as jnp
from jax import lax
from jax.experimental import pallas as pl
from jax.experimental.pallas import tpu as pltpu
from jax.sharding import PartitionSpec as P

SEG = 64
TOP = 2
EPS = 1e-06

LOG2E = 1.4426950408889634
MESH = pl.DeviceIdType.MESH
F32 = jnp.float32
BF16 = jnp.bfloat16


def dot_nt(left, right):
    return lax.dot_general(left, right, (((1,), (1,)), ((), ())), preferred_element_type=F32)


def remote(source, target, send_sem, recv_sem, axis, peer):
    return pltpu.make_async_remote_copy(
        src_ref=source,
        dst_ref=target,
        send_sem=send_sem,
        recv_sem=recv_sem,
        device_id={axis: peer},
        device_id_type=MESH,
    )


def greet(axes):
    barrier = pltpu.get_barrier_semaphore()
    total = 0
    for axis in axes:
        peers = lax.axis_size(axis)
        me = lax.axis_index(axis)
        for step in range(1, peers):
            pl.semaphore_signal(
                barrier, inc=1, device_id={axis: lax.rem(me + step, peers)}, device_id_type=MESH
            )
        total += peers - 1
    pl.semaphore_wait(barrier, total)


def columns_of(stats):
    repeat = stats.shape[1] // stats.shape[0]
    return jnp.concatenate([stats] * repeat, axis=0).T


def rows_of(columns):
    rows = columns[0].shape[0]
    lane = lax.broadcasted_iota(jnp.int32, (rows, rows), 1)
    tile = jnp.zeros((rows, rows), F32)
    for at, column in enumerate(columns):
        tile = jnp.where(lane == at, column, tile)
    return tile.T[: len(columns)]


class Refs:
    def __init__(self, names, refs):
        for name, ref in zip(names, refs):
            setattr(self, name, ref)


def attend(r, arrived):
    seq = lax.axis_size("sp")
    rows, heads, width_a = r.qa.shape
    width_b = r.qb.shape[2]
    value_a, value_b = r.va.shape[2], r.vb.shape[2]
    key_a, key_b = width_a // 2, width_b // 2
    chips = seq // 2
    half = chips // 2
    blocks = 2 * half
    spans = ((0, width_a), (width_a + value_a, width_a + value_a + width_b))
    factors = (key_a ** (-0.5) * LOG2E, key_b ** (-0.5) * LOG2E)
    lam, qa, ka, va, qb, kb, vb = r.lam, r.qa, r.ka, r.va, r.qb, r.kb, r.vb
    gain_a, gain_b, out_a, out_b = r.gain_a, r.gain_b, r.heads_a, r.heads_b
    kv, query, far_query, far_stats, own_stats = r.kv, r.query, r.far_query, r.far_stats, r.own_stats
    keep, part, far_part, total, far_total = r.keep, r.part, r.far_part, r.total, r.far_total
    chain_s, chain_r, part_s, part_r = r.chain_s, r.chain_r, r.part_s, r.part_r
    query_s, query_r, stats_s, stats_r = r.query_s, r.query_r, r.stats_s, r.stats_r
    back_s, back_r, total_s, total_r = r.back_s, r.back_r, r.total_s, r.total_r
    me = lax.axis_index("sp")
    chip, core = me // 2, lax.rem(me, 2)
    upper = chip >= half
    place = lax.rem(chip, half)
    base = chip - place
    middle = 2 * (half - 1) + core
    is_middle = chip == half - 1
    partner = 2 * chip + 1 - core
    above = jnp.minimum(me + 2, seq - 1 - (1 - core))
    slot = 2 * place + core

    def chain(y, head):
        ref = kv.at[2 * y + core, head]
        return remote(ref, ref, chain_s.at[y, head], chain_r.at[y, head], "sp", above)

    def across(y, head):
        ref = kv.at[2 * y + core, head]
        return remote(ref, ref, part_s.at[y, head], part_r.at[y, head], "sp", partner)

    def ask(head):
        return remote(
            query.at[head], far_query.at[place, head], query_s.at[head],
            query_r.at[place, head], "sp", middle,
        )

    def tell(head):
        return remote(
            own_stats.at[head], far_stats.at[place, head], stats_s.at[head],
            stats_r.at[place, head], "sp", middle,
        )

    def answer(i, head):
        return remote(
            part.at[i, head], far_part.at[head], back_s.at[i, head], back_r.at[head],
            "sp", 2 * (half + i) + core,
        )

    def answer_total(i, head):
        return remote(
            total.at[i, head], far_total.at[head], total_s.at[i, head], total_r.at[head],
            "sp", 2 * (half + i) + core,
        )

    def asked(i, head):
        return remote(
            query.at[head], far_query.at[i, head], query_s.at[head],
            query_r.at[i, head], "sp", middle,
        )

    def told(i, head):
        return remote(
            own_stats.at[head], far_stats.at[i, head], stats_s.at[head],
            stats_r.at[i, head], "sp", middle,
        )

    def pack(head):
        query[head, :, :width_a] = qa[:, head, :]
        query[head, :, width_a:] = qb[:, head, :]
        kv[slot, head, :, :width_a] = ka[:, head, :]
        kv[slot, head, :, spans[0][1] : spans[1][0]] = va[:, head, :]
        kv[slot, head, :, spans[1][0] : spans[1][1]] = kb[:, head, :]
        kv[slot, head, :, spans[1][1] :] = vb[:, head, :]

    arrived()
    for head in range(heads):
        pack(head)

        @pl.when(upper)
        def _():
            ask(head).start()

        @pl.when(place < half - 1)
        def _():
            chain(place, head).start()

        across(place, head).start()

    def gather(here, head):
        for y in range(here):
            chain(y, head).wait_recv()
            across(y, head).start()
            if here < half - 1:
                chain(y, head).start()
        for y in range(here + 1):
            across(y, head).wait_recv()

    def score_maps(ref, head, count):
        maps = []
        for group, (width, span) in enumerate(((width_a, spans[0][0]), (width_b, spans[1][0]))):
            begin = 0 if group == 0 else width_a
            wide = ref[:, begin : begin + width]
            block_keys = kv[:count, head, :, span : span + width].reshape(count * rows, width)
            size = width // 2
            if size % 128:
                lane = lax.broadcasted_iota(jnp.int32, wide.shape, 1)
                nothing = jnp.zeros_like(wide)
                first = dot_nt(jnp.where(lane < size, wide, nothing), block_keys)
                second = dot_nt(jnp.where(lane < size, nothing, wide), block_keys)
            else:
                first = dot_nt(wide[:, :size], block_keys[:, :size])
                second = dot_nt(wide[:, size:], block_keys[:, size:])
            maps += [first * factors[group], second * factors[group]]
        return maps

    def visible(count):
        query_seg = (
            slot * rows + lax.broadcasted_iota(jnp.int32, (rows, 1), 0)
        ) // SEG
        key_seg = lax.broadcasted_iota(jnp.int32, (1, count * rows), 1) // SEG
        return query_seg >= key_seg

    def combine(first, second, head, count, group):
        weights = (first - second).astype(BF16)
        begin = spans[group][1]
        size = value_a if group == 0 else value_b
        block_values = kv[:count, head, :, begin : begin + size].reshape(count * rows, size)
        return jnp.dot(weights, block_values, preferred_element_type=F32)

    def finish(mixed, gain, out, head, size):
        mean_sq = jnp.mean(mixed * mixed, axis=1, keepdims=True)
        value = (mixed * lax.rsqrt(mean_sq + EPS) * gain[...]).astype(BF16)
        out[:, pl.ds(pl.multiple_of(head * size, size), size)] = value

    def finish_both(mixed, head):
        finish(mixed[0], gain_a, out_a, head, value_a)
        finish(mixed[1], gain_b, out_b, head, value_b)

    def own_lower(head, count):
        seen = visible(count)
        maps = [jnp.where(seen, one, -jnp.inf) for one in score_maps(query.at[head], head, count)]
        mixed = []
        for group in range(2):
            parts = []
            for at in range(2):
                scores = maps[2 * group + at]
                expo = jnp.exp2(scores - jnp.max(scores, axis=1, keepdims=True))
                scale = 1.0 / jnp.sum(expo, axis=1, keepdims=True)
                if at:
                    scale = scale * lam[group, head]
                parts.append(expo * scale)
            mixed.append(combine(parts[0], parts[1], head, count, group))
        finish_both(mixed, head)

    def for_upper(i, head):
        asked(i, head).wait_recv()
        maps = score_maps(far_query.at[i, head], head, blocks)
        told(i, head).wait_recv()
        far = columns_of(far_stats[i, head])
        stats = []
        for group in range(2):
            parts = []
            for at in range(2):
                k = 2 * group + at
                scores = maps[k]
                far_max, far_sum = far[:, k : k + 1], far[:, 4 + k : 5 + k]
                top = jnp.maximum(jnp.max(scores, axis=1, keepdims=True), far_max)
                expo = jnp.exp2(scores - top)
                summed = jnp.sum(expo, axis=1, keepdims=True) + far_sum * jnp.exp2(far_max - top)
                stats.append((top, summed))
                scale = 1.0 / summed
                if at:
                    scale = scale * lam[group, head]
                parts.append(expo * scale)
            mixed = combine(parts[0], parts[1], head, blocks, group)
            begin = 0 if group == 0 else value_a
            part[i, head, :, begin : begin + mixed.shape[1]] = mixed.astype(BF16)
        answer(i, head).start()
        total[i, head] = rows_of([one[0] for one in stats] + [one[1] for one in stats])
        answer_total(i, head).start()

    def upper_first(head, count):
        seen = visible(count)
        maps = [jnp.where(seen, one, -jnp.inf) for one in score_maps(query.at[head], head, count)]
        tops, sums = [], []
        for k in range(4):
            top = jnp.max(maps[k], axis=1, keepdims=True)
            expo = jnp.exp2(maps[k] - top)
            keep[head, k, :, : count * rows] = expo
            tops.append(top)
            sums.append(jnp.sum(expo, axis=1, keepdims=True))
        own_stats[head] = rows_of(tops + sums)
        tell(head).start()

    def upper_second(head, count):
        answer_total(0, head).wait_recv()
        own = columns_of(own_stats[head])
        whole = columns_of(far_total[head])
        scales = []
        for k in range(4):
            scale = jnp.exp2(own[:, k : k + 1] - whole[:, k : k + 1]) / whole[:, 4 + k : 5 + k]
            if k % 2:
                scale = scale * lam[k // 2, head]
            scales.append(scale)
        mixed = []
        for group in range(2):
            first = keep[head, 2 * group, :, : count * rows] * scales[2 * group]
            second = keep[head, 2 * group + 1, :, : count * rows] * scales[2 * group + 1]
            mixed.append(combine(first, second, head, count, group))
        answer(0, head).wait_recv()
        far = far_part[head].astype(F32)
        finish_both([mixed[0] + far[:, :value_a], mixed[1] + far[:, value_a:]], head)

    for here in range(half):

        @pl.when((place == here) & jnp.logical_not(upper))
        def _():
            def step(head, carry):
                gather(here, head)
                own_lower(head, 2 * here + 2)
                if here == half - 1:

                    def each(i, inner):
                        for_upper(i, head)
                        return inner

                    lax.fori_loop(0, half, each, 0)
                return carry

            lax.fori_loop(0, heads, step, 0)

        @pl.when((place == here) & upper)
        def _():
            def step(head, carry):
                gather(here, head)
                upper_first(head, 2 * here + 2)
                return carry

            lax.fori_loop(0, heads, step, 0)

            def second(head, carry):
                upper_second(head, 2 * here + 2)
                return carry

            lax.fori_loop(0, heads, second, 0)

        @pl.when(place == here)
        def _():
            def drain(head, carry):
                for y in range(here + 1):
                    across(y, head).wait_send()
                    if here < half - 1:
                        chain(y, head).wait_send()
                return carry

            lax.fori_loop(0, heads, drain, 0)

    @pl.when(upper)
    def _():
        def drain(head, carry):
            ask(head).wait_send()
            tell(head).wait_send()
            return carry

        lax.fori_loop(0, heads, drain, 0)

    @pl.when(is_middle)
    def _():
        def drain(head, carry):
            for i in range(half):
                answer(i, head).wait_send()
                answer_total(i, head).wait_send()
            return carry

        lax.fori_loop(0, heads, drain, 0)


def grid_of(count):
    side = math.isqrt(count)
    return (side, side) if side * side == count else (1, count)


def peer_at(dy, dx):
    ny, nx = grid_of(lax.axis_size("tp"))
    me = lax.axis_index("tp")
    return lax.rem(me // nx + dy, ny) * nx + lax.rem(lax.rem(me, nx) + dx, nx)


def peer_offsets():
    ny, nx = grid_of(lax.axis_size("tp"))
    offsets = [(dy, dx) for dy in range(ny) for dx in range(nx) if dy or dx]
    far = lambda one: min(one[0], ny - one[0]) + min(one[1], nx - one[1])
    return sorted(offsets, key=far, reverse=True), ny, nx


def block_of(index, width):
    return pl.ds(pl.multiple_of(index * width, width), width)


def route(r):
    experts, slots, rows = r.select.shape
    square = (rows, rows)
    lane = lax.broadcasted_iota(jnp.int32, square, 1)
    line = lax.broadcasted_iota(jnp.int32, square, 0)
    named = r.routes[...]
    weight = r.route_weight[...]
    share = weight / jnp.sum(weight, axis=1, keepdims=True)
    chosen = jnp.zeros(square, F32)
    gate = jnp.zeros(square, F32)
    for k in range(TOP):
        match = named[:, k : k + 1] == lane
        chosen = chosen + jnp.where(match, 1.0, 0.0)
        gate = gate + jnp.where(match, share[:, k : k + 1], 0.0)
    chosen, gate = chosen.T, gate.T
    earlier = jnp.dot(
        chosen.astype(BF16),
        jnp.where(line < lane, 1.0, 0.0).astype(BF16),
        preferred_element_type=F32,
    )
    slot = lax.broadcasted_iota(jnp.int32, (slots, rows), 0).astype(F32)
    for expert in range(experts):
        pick = (chosen[expert : expert + 1] > 0.5) & (earlier[expert : expert + 1] == slot)
        r.select[expert] = jnp.where(pick, 1.0, 0.0).astype(BF16)
        r.weigh[expert * slots : (expert + 1) * slots, :] = jnp.where(
            pick, gate[expert : expert + 1], 0.0
        )
    weigh = r.weigh[...].T
    high = weigh.astype(BF16)
    r.high[...] = high
    r.low[...] = (weigh - high.astype(F32)).astype(BF16)


def project(r, loaded):
    offsets, _, _ = peer_offsets()
    me = lax.axis_index("tp")
    width = r.stream.shape[1]

    def piece(owner):
        columns = block_of(owner, width)
        return jnp.dot(
            r.heads_a[...], r.proj_a[:, columns], preferred_element_type=F32
        ) + jnp.dot(r.heads_b[...], r.proj_b[:, columns], preferred_element_type=F32)

    loaded()
    copies = []
    for at, offset in enumerate(offsets):
        peer = peer_at(*offset)
        r.branch_out[at] = piece(peer).astype(BF16)
        copy = remote(
            r.branch_out.at[at], r.branch_in.at[at], r.branch_s.at[at], r.branch_r.at[at], "tp", peer
        )
        copy.start()
        copies.append(copy)
    summed = piece(me)
    for at, copy in reversed(list(enumerate(copies))):
        copy.wait_recv()
        summed = summed + r.branch_in[at].astype(F32)
    r.stream[...] = (r.residual[...].astype(F32) + summed).astype(BF16)
    return copies


def experts_part(r, loaded):
    offsets, ny, nx = peer_offsets()
    seq, heads = lax.axis_size("sp"), lax.axis_size("tp")
    me, mine = lax.axis_index("sp"), lax.axis_index("tp")
    chips = seq // 2
    chip, core = me // 2, lax.rem(me, 2)
    experts, slots, rows = r.select.shape
    width = r.stream.shape[1]
    square = ny == 2 and nx == 2
    across_x, across_y, across_both = peer_at(0, 1), peer_at(1, 0), peer_at(1, 1)
    top, bottom = pl.ds(0, slots), pl.ds(slots, slots)

    def source(step):
        return lax.rem(chip + chips - step, chips)

    def outgoing(step, side):
        target_core = core if side == 0 else 1 - core
        expert = 2 * lax.rem(chip + step, chips) + target_core
        return expert, remote(
            r.send.at[expert],
            r.rows.at[chip, block_of(core, slots), block_of(mine, width)],
            r.out_s.at[step, side],
            r.out_r.at[step, side],
            "sp",
            expert,
        )

    for step in range(chips):
        for side in range(2):
            expert, copy = outgoing(step, side)
            picked = jnp.dot(r.select[expert], r.stream[...], preferred_element_type=F32)
            if step == 0 and side == 0:
                r.rows[chip, block_of(core, slots), block_of(mine, width)] = picked.astype(BF16)
            else:
                r.send[expert] = picked.astype(BF16)
                copy.start()

    def incoming(step, side):
        origin_core = core if side == 0 else 1 - core
        origin = source(step)
        return remote(
            r.send.at[me],
            r.rows.at[origin, block_of(origin_core, slots), block_of(mine, width)],
            r.out_s.at[step, side],
            r.out_r.at[step, side],
            "sp",
            2 * origin + origin_core,
        )

    def land(step):
        @pl.when(step > 0)
        def _():
            incoming(step, 0).wait_recv()

        incoming(step, 1).wait_recv()

    def spread(step, at, peer, owner):
        ref = r.rows.at[source(step), :, block_of(owner, width)]
        return remote(ref, ref, r.spread_s.at[step, at], r.spread_r.at[step, at], "tp", peer)

    def relay(step, at, peer, owner):
        ref = r.rows.at[source(step), top if at == 0 else bottom, block_of(owner, width)]
        return remote(ref, ref, r.relay_s.at[step, at], r.relay_r.at[step, at], "tp", peer)

    near = ((0, 1), (1, 0)) if square else offsets

    def start_spread(step):
        land(step)
        for at, offset in enumerate(near):
            spread(step, at, peer_at(*offset), mine).start()

    def start_relay(step):
        for at, offset in enumerate(near):
            giver = peer_at(ny - offset[0], nx - offset[1])
            spread(step, at, giver, giver).wait_recv()
        if square:
            relay(step, 0, across_y, across_x).start()
            relay(step, 1, across_x, across_y).start()

    def compute(step):
        if square:
            relay(step, 0, across_y, across_both).wait_recv()
            relay(step, 1, across_x, across_both).wait_recv()
        origin = source(step)
        wide = r.rows[origin].astype(F32)
        mean_sq = jnp.mean(wide * wide, axis=1, keepdims=True)
        normed = (wide * lax.rsqrt(mean_sq + EPS) * r.norm_gain[...]).astype(BF16)
        gate = jnp.dot(normed, r.gate[...], preferred_element_type=F32)
        up = jnp.dot(normed, r.up[...], preferred_element_type=F32)
        hidden = (gate / (1.0 + jnp.exp(-gate)) * up).astype(BF16)
        r.down_out[step] = jnp.dot(hidden, r.down[...], preferred_element_type=F32).astype(BF16)

    def first_copies(step):
        if not square:
            return [
                remote(
                    r.down_out.at[step, :, block_of(peer_at(*offset), width)],
                    r.first.at[step, at],
                    r.first_s.at[step, at],
                    r.first_r.at[step, at],
                    "tp",
                    peer_at(*offset),
                )
                for at, offset in enumerate(offsets)
            ]
        plan = (
            (top, across_x, across_both, 1),
            (bottom, across_y, across_both, 3),
            (top, across_x, across_x, 0),
            (bottom, across_y, across_y, 2),
        )
        return [
            remote(
                r.down_out.at[step, part, block_of(owner, width)],
                r.first.at[step, slot],
                r.first_s.at[step, slot],
                r.first_r.at[step, slot],
                "tp",
                peer,
            )
            for part, peer, owner, slot in plan
        ]

    def second_copies(step):
        return [
            remote(
                r.second_out.at[step, at],
                r.second.at[step, at],
                r.second_s.at[step, at],
                r.second_r.at[step, at],
                "tp",
                peer,
            )
            for at, peer in enumerate((across_y, across_x))
        ]

    def start_first(step):
        for copy in first_copies(step):
            copy.start()

    def start_second(step):
        if not square:
            return
        firsts, seconds = first_copies(step), second_copies(step)
        for at, part, owner, slot in ((0, top, across_y, 1), (1, bottom, across_x, 3)):
            firsts[at].wait_recv()
            summed = r.down_out[step, part, block_of(owner, width)].astype(F32)
            summed = summed + r.first[step, slot].astype(F32)
            r.second_out[step, at] = summed.astype(BF16)
            seconds[at].start()

    def home(step, side):
        origin_core = core if side == 0 else 1 - core
        return remote(
            r.summed.at[step, side],
            r.back.at[me],
            r.home_s.at[step, side],
            r.home_r.at[step, side],
            "sp",
            2 * source(step) + origin_core,
        )

    def returned(step, side):
        expert_core = core if side == 0 else 1 - core
        expert = 2 * lax.rem(chip + step, chips) + expert_core
        return remote(
            r.summed.at[step, side],
            r.back.at[expert],
            r.home_s.at[step, side],
            r.home_r.at[step, side],
            "sp",
            expert,
        )

    def start_home(step):
        own = block_of(mine, width)
        firsts = first_copies(step)
        if square:
            seconds = second_copies(step)
            firsts[2].wait_recv()
            firsts[3].wait_recv()
            halves = []
            for at, part, slot in ((0, top, 0), (1, bottom, 2)):
                seconds[at].wait_recv()
                halves.append(
                    r.down_out[step, part, own].astype(F32)
                    + r.first[step, slot].astype(F32)
                    + r.second[step, at].astype(F32)
                )
            r.sums[0] = halves[0].astype(BF16)
            r.sums[1] = halves[1].astype(BF16)
        else:
            summed = r.down_out[step, :, own].astype(F32)
            for at, copy in enumerate(firsts):
                copy.wait_recv()
                summed = summed + r.first[step, at].astype(F32)
            r.sums[0] = summed[:slots].astype(BF16)
            r.sums[1] = summed[slots:].astype(BF16)
        r.summed[step, 0] = r.sums[core]
        r.summed[step, 1] = r.sums[1 - core]

        @pl.when(step == 0)
        def _():
            r.back[me] = r.summed[0, 0]

        @pl.when(step > 0)
        def _():
            home(step, 0).start()

        home(step, 1).start()

    loaded()
    start_spread(0)
    if chips > 1:
        start_spread(1)
    start_relay(0)

    def body(step, carry):
        @pl.when(step + 2 < chips)
        def _():
            start_spread(step + 2)

        @pl.when(step + 1 < chips)
        def _():
            start_relay(step + 1)

        @pl.when(step < chips)
        def _():
            compute(step)
            start_first(step)

        @pl.when((step >= 1) & (step < chips + 1))
        def _():
            start_second(step - 1)

        @pl.when(step >= 2)
        def _():
            start_home(step - 2)

        return carry

    lax.fori_loop(0, chips + 2, body, 0)

    def arrive(step, carry):
        @pl.when(step > 0)
        def _():
            returned(step, 0).wait_recv()

        returned(step, 1).wait_recv()
        return carry

    lax.fori_loop(0, chips, arrive, 0)
    back = r.back[...].reshape(experts * slots, width)
    mixed = jnp.dot(r.high[...], back, preferred_element_type=F32)
    mixed = mixed + jnp.dot(r.low[...], back, preferred_element_type=F32)
    r.out[...] = (r.stream[...].astype(F32) + mixed).astype(BF16)

    def drain(step, carry):
        @pl.when(step > 0)
        def _():
            outgoing(step, 0)[1].wait_send()
            home(step, 0).wait_send()

        outgoing(step, 1)[1].wait_send()
        home(step, 1).wait_send()
        for at, offset in enumerate(near):
            spread(step, at, peer_at(*offset), mine).wait_send()
        if square:
            relay(step, 0, across_y, across_x).wait_send()
            relay(step, 1, across_x, across_y).wait_send()
            for copy in second_copies(step):
                copy.wait_send()
        for copy in first_copies(step):
            copy.wait_send()
        return carry

    lax.fori_loop(0, chips, drain, 0)


def layer(args):
    seq, heads_dev = lax.axis_size("sp"), lax.axis_size("tp")
    rows, heads, width_a = args["qa"].shape
    width_b = args["qb"].shape[2]
    value_a, value_b = args["va"].shape[2], args["vb"].shape[2]
    model = args["residual"].shape[1]
    width = model // heads_dev
    chips = seq // 2
    half = chips // 2
    blocks = 2 * half
    slots = 2 * rows * TOP // seq
    _, ny, nx = peer_offsets()
    square = ny == 2 and nx == 2
    spreads = 2 if square else heads_dev - 1
    first_shape = (4, slots, width) if square else (heads_dev - 1, 2 * slots, width)
    dma = pltpu.SemaphoreType.DMA
    big = ("qa", "ka", "va", "qb", "kb", "vb", "residual", "proj_a", "proj_b", "gate", "up", "down")
    small = ("lam", "gain_a", "gain_b", "norm_gain", "routes", "route_weight")

    def landing(name):
        shape = args[name].shape
        if name == "residual":
            shape = (rows, width)
        if len(shape) == 3 and name in ("gate", "up", "down"):
            shape = shape[1:]
        return pltpu.VMEM(shape, args[name].dtype)

    scratch = {name: landing(name) for name in big}
    scratch.update(
        load_s=dma((len(big),)),
        heads_a=pltpu.VMEM((rows, heads * value_a), BF16),
        heads_b=pltpu.VMEM((rows, heads * value_b), BF16),
        kv=pltpu.VMEM((blocks, heads, rows, width_a + value_a + width_b + value_b), BF16),
        query=pltpu.VMEM((heads, rows, width_a + width_b), BF16),
        far_query=pltpu.VMEM((half, heads, rows, width_a + width_b), BF16),
        far_stats=pltpu.VMEM((half, heads, 8, rows), F32),
        own_stats=pltpu.VMEM((heads, 8, rows), F32),
        keep=pltpu.VMEM((heads, 4, rows, blocks * rows), F32),
        part=pltpu.VMEM((half, heads, rows, value_a + value_b), BF16),
        far_part=pltpu.VMEM((heads, rows, value_a + value_b), BF16),
        total=pltpu.VMEM((half, heads, 8, rows), F32),
        far_total=pltpu.VMEM((heads, 8, rows), F32),
        chain_s=dma((half, heads)), chain_r=dma((half, heads)),
        part_s=dma((half, heads)), part_r=dma((half, heads)),
        query_s=dma((heads,)), query_r=dma((half, heads)),
        stats_s=dma((heads,)), stats_r=dma((half, heads)),
        back_s=dma((half, heads)), back_r=dma((heads,)),
        total_s=dma((half, heads)), total_r=dma((heads,)),
        branch_out=pltpu.VMEM((heads_dev - 1, rows, width), BF16),
        branch_in=pltpu.VMEM((heads_dev - 1, rows, width), BF16),
        branch_s=dma((heads_dev - 1,)), branch_r=dma((heads_dev - 1,)),
        stream=pltpu.VMEM((rows, width), BF16),
        select=pltpu.VMEM((seq, slots, rows), BF16),
        weigh=pltpu.VMEM((seq * slots, rows), F32),
        high=pltpu.VMEM((rows, seq * slots), BF16),
        low=pltpu.VMEM((rows, seq * slots), BF16),
        send=pltpu.VMEM((seq, slots, width), BF16),
        rows=pltpu.VMEM((chips, 2 * slots, model), BF16),
        out_s=dma((chips, 2)), out_r=dma((chips, 2)),
        spread_s=dma((chips, spreads)), spread_r=dma((chips, spreads)),
        relay_s=dma((chips, 2)), relay_r=dma((chips, 2)),
        down_out=pltpu.VMEM((chips, 2 * slots, model), BF16),
        first=pltpu.VMEM((chips,) + first_shape, BF16),
        first_s=dma((chips, first_shape[0])), first_r=dma((chips, first_shape[0])),
        second_out=pltpu.VMEM((chips, 2, slots, width), BF16),
        second=pltpu.VMEM((chips, 2, slots, width), BF16),
        second_s=dma((chips, 2)), second_r=dma((chips, 2)),
        sums=pltpu.VMEM((2, slots, width), BF16),
        summed=pltpu.VMEM((chips, 2, slots, width), BF16),
        back=pltpu.VMEM((seq, slots, width), BF16),
        home_s=dma((chips, 2)), home_r=dma((chips, 2)),
    )

    def kernel(*refs):
        small_refs = refs[: len(small)]
        hbm = Refs(big, refs[len(small) : len(small) + len(big)])
        at = len(small) + len(big)
        r = Refs(
            small + ("out",) + tuple(scratch), tuple(small_refs) + (refs[at],) + tuple(refs[at + 1 :])
        )

        def load(name):
            source = getattr(hbm, name)
            if name == "residual":
                source = source.at[:, block_of(lax.axis_index("tp"), width)]
            if name in ("gate", "up", "down"):
                source = source.at[0]
            return pltpu.make_async_copy(source, getattr(r, name), r.load_s.at[big.index(name)])

        def wait(*names):
            for name in names:
                load(name).wait()

        for name in big:
            load(name).start()
        greet(("sp", "tp"))
        attend(r, lambda: wait("qa", "ka", "va", "qb", "kb", "vb"))
        route(r)
        copies = project(r, lambda: wait("residual", "proj_a", "proj_b"))
        experts_part(r, lambda: wait("gate", "up", "down"))
        for copy in copies:
            copy.wait_send()

    vmem = pl.BlockSpec(memory_space=pltpu.VMEM)
    specs = [pl.BlockSpec(memory_space=pltpu.SMEM)] + [vmem] * (len(small) - 1)
    specs += [pl.BlockSpec(memory_space=pl.ANY)] * len(big)
    return pl.pallas_call(
        kernel,
        out_shape=jax.ShapeDtypeStruct((rows, width), BF16),
        in_specs=specs,
        out_specs=vmem,
        scratch_shapes=list(scratch.values()),
        compiler_params=pltpu.CompilerParams(
            collective_id=0, has_side_effects=True, vmem_limit_bytes=56 * 2**20
        ),
        name="layer",
    )(*[args[name] for name in small + big])


def local(
    residual,
    query_a,
    keys_a,
    values_a,
    query_b,
    keys_b,
    values_b,
    lambda_a,
    lambda_b,
    gain_a,
    gain_b,
    proj_a,
    proj_b,
    norm_gain,
    routes,
    route_weight,
    expert_gate,
    expert_up,
    expert_down,
):
    args = dict(
        residual=residual,
        qa=query_a,
        ka=keys_a,
        va=values_a,
        qb=query_b,
        kb=keys_b,
        vb=values_b,
        lam=jnp.stack([lambda_a, lambda_b]),
        gain_a=gain_a.reshape(1, -1),
        gain_b=gain_b.reshape(1, -1),
        proj_a=proj_a,
        proj_b=proj_b,
        norm_gain=norm_gain.reshape(1, -1),
        routes=routes,
        route_weight=route_weight,
        gate=expert_gate,
        up=expert_up,
        down=expert_down,
    )
    return layer(args)


def solution(mesh):
    placed = (
        P("sp", None),
        P("sp", "tp", None),
        P("sp", "tp", None),
        P("sp", "tp", None),
        P("sp", "tp", None),
        P("sp", "tp", None),
        P("sp", "tp", None),
        P("tp"),
        P("tp"),
        P(),
        P(),
        P("tp", None),
        P("tp", None),
        P(),
        P("sp", None),
        P("sp", None),
        P("sp", None, "tp"),
        P("sp", None, "tp"),
        P("sp", "tp", None),
    )
    return jax.shard_map(
        local, mesh=mesh, in_specs=placed, out_specs=P("sp", "tp"), check_vma=False
    )
```

time: 224 us -> 117 us (0.52)
  the two profiles are of different devices: /device:TPU:25 before, /device:TPU:0 now
where the time goes in v2:
time: 117 us
  Pallas kernels  111 us (95%)
  local copies, waits for them, and re-layouts  4.38 us (4%)
  other arithmetic  1.25 us (1%)
    pallas_call x1, Pallas kernels, layer(): pl.pallas_call(kernel, out_shape=jax.ShapeDtypeStruct((rows, width), BF16...  111 us
    unnamed x3, local copies, waits for them, and re-layouts  4.38 us

profile of v2, /device:TPU:0, one launch (start us, length us, event | category | flops | bytes accessed | tf_op | source)
XLA Modules:
  0.0 116.9 jit_solution(2991703885800553173)
XLA Ops:
  0.0 1.3 %pad_maximum_fusion.refs_0_ = f32[2,4]{1,0:T(2,128)} fusion(f32[1,4]{1,0:T(1,128)} %bitcast.8, f32[1,4]{1,0:T(1,128)} %bitcast.9), kind=kLoop, calls=%fused_computation | loop fusion | flops 8 | bytes 64 | tf_op jit(solution)/shard_map/stack | solution.py:864
  1.3 1.4 %copy.20.refs_4_ = s32[128,2]{1,0:T(8,128)} copy(s32[128,2]{0,1:T(2,128)} %param.33) | data formatting | bytes 2048 | tf_op args[14]
  2.7 1.4 %copy.21.refs_5_ = f32[128,2]{1,0:T(8,128)} copy(f32[128,2]{0,1:T(2,128)} %param.34) | data formatting | bytes 2048 | tf_op args[15]
  4.1 111.2 %layer.1 = bf16[128,512]{1,0:T(8,128)(2,1)} custom-call(f32[2,4]{1,0:T(2,128)} %pad_maximum_fusion.refs_0_, f32[1,128]{1,0:T(1,128)} %bitcast.7, f32[1,256]{1,0:T(1,128)} %bitcast.6, f32[1,2048]{1,0:T(1,128)} %bitcast.5, s32[128,2]{1,0:T(8,128)} %copy.20.refs_4_, f32[128,2]{1,0:T(8,128)} %copy.21.refs_5_, bf16[128,4,128]{2,1,0:T(4,128)(2,1)} %refs_6_.1, ...), custom_call_target="tpu_custom_call" | custom-call | tf_op jit(solution)/shard_map/layer/pallas_call | solution.py:822
  115.3 1.6 %copy.23 = bf16[128,512]{1,0:T(8,128)(2,1)} copy(bf16[128,512]{1,0:T(8,128)(2,1)} %layer.1) | data formatting | bytes 262144

commit v3 on v2

--- a/solution.py
+++ b/solution.py
@@ -43,7 +43,7 @@
                 barrier, inc=1, device_id={axis: lax.rem(me + step, peers)}, device_id_type=MESH
             )
         total += peers - 1
-    pl.semaphore_wait(barrier, total)
+    return lambda: pl.semaphore_wait(barrier, total)
 
 
 def columns_of(stats):
@@ -66,7 +66,7 @@
             setattr(self, name, ref)
 
 
-def attend(r, arrived):
+def attend(r, arrived, greeted, meanwhile):
     seq = lax.axis_size("sp")
     rows, heads, width_a = r.qa.shape
     width_b = r.qb.shape[2]
@@ -75,107 +75,114 @@
     chips = seq // 2
     half = chips // 2
     blocks = 2 * half
-    spans = ((0, width_a), (width_a + value_a, width_a + value_a + width_b))
+    pair = 2 - half % 2
+    wide_q = width_a + width_b
+    key_spans = ((0, width_a), (width_a, width_b))
+    value_spans = ((wide_q, value_a), (wide_q + value_a, value_b))
+    parts_of = (pl.ds(0, wide_q), pl.ds(wide_q, value_a + value_b))
     factors = (key_a ** (-0.5) * LOG2E, key_b ** (-0.5) * LOG2E)
-    lam, qa, ka, va, qb, kb, vb = r.lam, r.qa, r.ka, r.va, r.qb, r.kb, r.vb
-    gain_a, gain_b, out_a, out_b = r.gain_a, r.gain_b, r.heads_a, r.heads_b
-    kv, query, far_query, far_stats, own_stats = r.kv, r.query, r.far_query, r.far_stats, r.own_stats
-    keep, part, far_part, total, far_total = r.keep, r.part, r.far_part, r.total, r.far_total
-    chain_s, chain_r, part_s, part_r = r.chain_s, r.chain_r, r.part_s, r.part_r
-    query_s, query_r, stats_s, stats_r = r.query_s, r.query_r, r.stats_s, r.stats_r
-    back_s, back_r, total_s, total_r = r.back_s, r.back_r, r.total_s, r.total_r
+    lams = (r.lam_a, r.lam_b)
+    kv, query = r.kv, r.query
+
     me = lax.axis_index("sp")
     chip, core = me // 2, lax.rem(me, 2)
     upper = chip >= half
+    lower = chip < half
     place = lax.rem(chip, half)
-    base = chip - place
     middle = 2 * (half - 1) + core
-    is_middle = chip == half - 1
     partner = 2 * chip + 1 - core
-    above = jnp.minimum(me + 2, seq - 1 - (1 - core))
+    above = jnp.minimum(me + 2, seq - 2 + core)
     slot = 2 * place + core
 
-    def chain(y, head):
-        ref = kv.at[2 * y + core, head]
-        return remote(ref, ref, chain_s.at[y, head], chain_r.at[y, head], "sp", above)
-
-    def across(y, head):
-        ref = kv.at[2 * y + core, head]
-        return remote(ref, ref, part_s.at[y, head], part_r.at[y, head], "sp", partner)
-
-    def ask(head):
+    def chain(y, head, part):
+        ref = kv.at[2 * y + core, head, :, parts_of[part]]
         return remote(
-            query.at[head], far_query.at[place, head], query_s.at[head],
-            query_r.at[place, head], "sp", middle,
-        )
-
-    def tell(head):
+            ref, ref, r.chain_s.at[y, head, part], r.chain_r.at[y, head, part], "sp", above
+        )
+
+    def across(y, head, part):
+        ref = kv.at[2 * y + core, head, :, parts_of[part]]
         return remote(
-            own_stats.at[head], far_stats.at[place, head], stats_s.at[head],
-            stats_r.at[place, head], "sp", middle,
+            ref, ref, r.part_s.at[y, head, part], r.part_r.at[y, head, part], "sp", partner
+        )
+
+    def ask(i, head):
+        return remote(
+            query.at[head], r.far_query.at[i, head], r.query_s.at[head], r.query_r.at[i, head],
+            "sp", middle,
+        )
+
+    def tell(i, head):
+        return remote(
+            r.own_stats.at[head], r.far_stats.at[i, head], r.stats_s.at[head],
+            r.stats_r.at[i, head], "sp", middle,
         )
 
     def answer(i, head):
         return remote(
-            part.at[i, head], far_part.at[head], back_s.at[i, head], back_r.at[head],
+            r.part.at[i, head], r.far_part.at[head], r.back_s.at[i, head], r.back_r.at[head],
             "sp", 2 * (half + i) + core,
         )
 
     def answer_total(i, head):
         return remote(
-            total.at[i, head], far_total.at[head], total_s.at[i, head], total_r.at[head],
+            r.total.at[i, head], r.far_total.at[head], r.total_s.at[i, head], r.total_r.at[head],
             "sp", 2 * (half + i) + core,
         )
 
-    def asked(i, head):
-        return remote(
-            query.at[head], far_query.at[i, head], query_s.at[head],
-            query_r.at[i, head], "sp", middle,
-        )
-
-    def told(i, head):
-        return remote(
-            own_stats.at[head], far_stats.at[i, head], stats_s.at[head],
-            stats_r.at[i, head], "sp", middle,
-        )
-
     def pack(head):
-        query[head, :, :width_a] = qa[:, head, :]
-        query[head, :, width_a:] = qb[:, head, :]
-        kv[slot, head, :, :width_a] = ka[:, head, :]
-        kv[slot, head, :, spans[0][1] : spans[1][0]] = va[:, head, :]
-        kv[slot, head, :, spans[1][0] : spans[1][1]] = kb[:, head, :]
-        kv[slot, head, :, spans[1][1] :] = vb[:, head, :]
+        query[head, :, :width_a] = r.qa[:, head, :]
+        query[head, :, width_a:] = r.qb[:, head, :]
+        for span, ref in zip(key_spans + value_spans, (r.ka, r.kb, r.va, r.vb)):
+            kv[slot, head, :, span[0] : span[0] + span[1]] = ref[:, head, :]
 
     arrived()
     for head in range(heads):
         pack(head)
-
-        @pl.when(upper)
-        def _():
-            ask(head).start()
-
+    greeted()
+
+    def give(head, part):
         @pl.when(place < half - 1)
         def _():
-            chain(place, head).start()
-
-        across(place, head).start()
-
-    def gather(here, head):
+            chain(place, head, part).start()
+
+        across(place, head, part).start()
+
+    @pl.when(upper)
+    def _():
+        for head in range(heads):
+            if head == 0:
+                ask(place, head).start()
+            give(head, 0)
+        for head in range(heads):
+            give(head, 1)
+
+    @pl.when(lower)
+    def _():
+        for head in range(heads):
+            give(head, 0)
+            give(head, 1)
+
+    def pass_on(here, head, part):
         for y in range(here):
-            chain(y, head).wait_recv()
-            across(y, head).start()
+            chain(y, head, part).wait_recv()
+            across(y, head, part).start()
             if here < half - 1:
-                chain(y, head).start()
+                chain(y, head, part).start()
+
+    def landed(here, head, part):
         for y in range(here + 1):
-            across(y, head).wait_recv()
-
-    def score_maps(ref, head, count):
+            across(y, head, part).wait_recv()
+
+    def gather(here, head, part):
+        pass_on(here, head, part)
+        landed(here, head, part)
+
+    def score_maps(queries, head, count):
         maps = []
-        for group, (width, span) in enumerate(((width_a, spans[0][0]), (width_b, spans[1][0]))):
-            begin = 0 if group == 0 else width_a
-            wide = ref[:, begin : begin + width]
-            block_keys = kv[:count, head, :, span : span + width].reshape(count * rows, width)
+        for group, (begin, width) in enumerate(key_spans):
+            wide = queries[:, begin : begin + width]
+            block_keys = kv[:count, head, :, begin : begin + width].reshape(count * rows, width)
             size = width // 2
             if size % 128:
                 lane = lax.broadcasted_iota(jnp.int32, wide.shape, 1)
@@ -189,16 +196,13 @@
         return maps
 
     def visible(count):
-        query_seg = (
-            slot * rows + lax.broadcasted_iota(jnp.int32, (rows, 1), 0)
-        ) // SEG
+        query_seg = (slot * rows + lax.broadcasted_iota(jnp.int32, (rows, 1), 0)) // SEG
         key_seg = lax.broadcasted_iota(jnp.int32, (1, count * rows), 1) // SEG
         return query_seg >= key_seg
 
     def combine(first, second, head, count, group):
         weights = (first - second).astype(BF16)
-        begin = spans[group][1]
-        size = value_a if group == 0 else value_b
+        begin, size = value_spans[group]
         block_values = kv[:count, head, :, begin : begin + size].reshape(count * rows, size)
         return jnp.dot(weights, block_values, preferred_element_type=F32)
 
@@ -208,8 +212,8 @@
         out[:, pl.ds(pl.multiple_of(head * size, size), size)] = value
 
     def finish_both(mixed, head):
-        finish(mixed[0], gain_a, out_a, head, value_a)
-        finish(mixed[1], gain_b, out_b, head, value_b)
+        finish(mixed[0], r.gain_a, r.heads_a, head, value_a)
+        finish(mixed[1], r.gain_b, r.heads_b, head, value_b)
 
     def own_lower(head, count):
         seen = visible(count)
@@ -222,37 +226,50 @@
                 expo = jnp.exp2(scores - jnp.max(scores, axis=1, keepdims=True))
                 scale = 1.0 / jnp.sum(expo, axis=1, keepdims=True)
                 if at:
-                    scale = scale * lam[group, head]
+                    scale = scale * lams[group][head]
                 parts.append(expo * scale)
             mixed.append(combine(parts[0], parts[1], head, count, group))
         finish_both(mixed, head)
 
+    def wait_far(i, head):
+        for at in range(pair):
+            ask(i + at, head).wait_recv()
+        for at in range(pair):
+            tell(i + at, head).wait_recv()
+
     def for_upper(i, head):
-        asked(i, head).wait_recv()
-        maps = score_maps(far_query.at[i, head], head, blocks)
-        told(i, head).wait_recv()
-        far = columns_of(far_stats[i, head])
-        stats = []
+        queries = r.far_query[pl.ds(i, pair), head].reshape(pair * rows, wide_q)
+        maps = score_maps(queries, head, blocks)
+        far = jnp.concatenate(
+            [columns_of(r.far_stats[i + at, head]) for at in range(pair)], axis=0
+        )
+        stats, expos, scales = [], [], []
+        for k in range(4):
+            far_max, far_sum = far[:, k : k + 1], far[:, 4 + k : 5 + k]
+            own_max = jnp.max(maps[k], axis=1, keepdims=True)
+            expo = jnp.exp2(maps[k] - own_max)
+            top = jnp.maximum(own_max, far_max)
+            down = jnp.exp2(own_max - top)
+            summed = jnp.sum(expo, axis=1, keepdims=True) * down + far_sum * jnp.exp2(far_max - top)
+            stats.append((top, summed))
+            expos.append(expo)
+            scales.append(down / summed)
         for group in range(2):
-            parts = []
-            for at in range(2):
-                k = 2 * group + at
-                scores = maps[k]
-                far_max, far_sum = far[:, k : k + 1], far[:, 4 + k : 5 + k]
-                top = jnp.maximum(jnp.max(scores, axis=1, keepdims=True), far_max)
-                expo = jnp.exp2(scores - top)
-                summed = jnp.sum(expo, axis=1, keepdims=True) + far_sum * jnp.exp2(far_max - top)
-                stats.append((top, summed))
-                scale = 1.0 / summed
-                if at:
-                    scale = scale * lam[group, head]
-                parts.append(expo * scale)
-            mixed = combine(parts[0], parts[1], head, blocks, group)
-            begin = 0 if group == 0 else value_a
-            part[i, head, :, begin : begin + mixed.shape[1]] = mixed.astype(BF16)
-        answer(i, head).start()
-        total[i, head] = rows_of([one[0] for one in stats] + [one[1] for one in stats])
-        answer_total(i, head).start()
+            first = expos[2 * group] * scales[2 * group]
+            second = expos[2 * group + 1] * (lams[group][head] * scales[2 * group + 1])
+            mixed = combine(first, second, head, blocks, group)
+            begin, size = (0, value_a) if group == 0 else (value_a, value_b)
+            r.part[pl.ds(i, pair), head, :, begin : begin + size] = mixed.astype(BF16).reshape(
+                pair, rows, size
+            )
+        for at in range(pair):
+            part = slice(at * rows, (at + 1) * rows)
+            r.total[i + at, head] = rows_of(
+                [one[0][part] for one in stats] + [one[1][part] for one in stats]
+            )
+        for at in reversed(range(pair)):
+            answer_total(i + at, head).start()
+            answer(i + at, head).start()
 
     def upper_first(head, count):
         seen = visible(count)
@@ -261,45 +278,68 @@
         for k in range(4):
             top = jnp.max(maps[k], axis=1, keepdims=True)
             expo = jnp.exp2(maps[k] - top)
-            keep[head, k, :, : count * rows] = expo
+            r.keep[head, k, :, : count * rows] = expo
             tops.append(top)
             sums.append(jnp.sum(expo, axis=1, keepdims=True))
-        own_stats[head] = rows_of(tops + sums)
-        tell(head).start()
+        r.own_stats[head] = rows_of(tops + sums)
+        tell(place, head).start()
 
     def upper_second(head, count):
         answer_total(0, head).wait_recv()
-        own = columns_of(own_stats[head])
-        whole = columns_of(far_total[head])
+        own = columns_of(r.own_stats[head])
+        whole = columns_of(r.far_total[head])
         scales = []
         for k in range(4):
             scale = jnp.exp2(own[:, k : k + 1] - whole[:, k : k + 1]) / whole[:, 4 + k : 5 + k]
             if k % 2:
-                scale = scale * lam[k // 2, head]
+                scale = scale * lams[k // 2][head]
             scales.append(scale)
         mixed = []
         for group in range(2):
-            first = keep[head, 2 * group, :, : count * rows] * scales[2 * group]
-            second = keep[head, 2 * group + 1, :, : count * rows] * scales[2 * group + 1]
+            first = r.keep[head, 2 * group, :, : count * rows] * scales[2 * group]
+            second = r.keep[head, 2 * group + 1, :, : count * rows] * scales[2 * group + 1]
             mixed.append(combine(first, second, head, count, group))
         answer(0, head).wait_recv()
-        far = far_part[head].astype(F32)
+        far = r.far_part[head].astype(F32)
         finish_both([mixed[0] + far[:, :value_a], mixed[1] + far[:, value_a:]], head)
 
     for here in range(half):
 
-        @pl.when((place == here) & jnp.logical_not(upper))
+        @pl.when((place == here) & lower)
         def _():
+            meanwhile()
+
+            pass_on(here, 0, 0)
+            pass_on(here, 0, 1)
+
             def step(head, carry):
-                gather(here, head)
-                own_lower(head, 2 * here + 2)
+                landed(here, head, 0)
+                landed(here, head, 1)
                 if here == half - 1:
 
                     def each(i, inner):
-                        for_upper(i, head)
+                        wait_far(i * pair, head)
+                        for_upper(i * pair, head)
                         return inner
 
-                    lax.fori_loop(0, half, each, 0)
+                    lax.fori_loop(1, half // pair, each, 0)
+                    wait_far(0, head)
+                    own_lower(head, 2 * here + 2)
+                    for_upper(0, head)
+                else:
+                    own_lower(head, 2 * here + 2)
+                if here:
+
+                    @pl.when((head == 0) & (heads > 1))
+                    def _():
+                        pass_on(here, min(1, heads - 1), 0)
+                        pass_on(here, min(1, heads - 1), 1)
+
+                    @pl.when(head + 2 < heads)
+                    def _():
+                        pass_on(here, head + 2, 0)
+                        pass_on(here, head + 2, 1)
+
                 return carry
 
             lax.fori_loop(0, heads, step, 0)
@@ -307,11 +347,23 @@
         @pl.when((place == here) & upper)
         def _():
             def step(head, carry):
-                gather(here, head)
+                gather(here, head, 0)
                 upper_first(head, 2 * here + 2)
+
+                @pl.when(head + 1 < heads)
+                def _():
+                    ask(place, head + 1).start()
+
                 return carry
 
             lax.fori_loop(0, heads, step, 0)
+            meanwhile()
+
+            def rest(head, carry):
+                gather(here, head, 1)
+                return carry
+
+            lax.fori_loop(0, heads, rest, 0)
 
             def second(head, carry):
                 upper_second(head, 2 * here + 2)
@@ -319,35 +371,40 @@
 
             lax.fori_loop(0, heads, second, 0)
 
-        @pl.when(place == here)
+    def drain():
+        for here in range(half):
+
+            @pl.when(place == here)
+            def _():
+                def each(head, carry):
+                    for y in range(here + 1):
+                        for part in range(2):
+                            across(y, head, part).wait_send()
+                            if here < half - 1:
+                                chain(y, head, part).wait_send()
+                    return carry
+
+                lax.fori_loop(0, heads, each, 0)
+
+        @pl.when(upper)
         def _():
-            def drain(head, carry):
-                for y in range(here + 1):
-                    across(y, head).wait_send()
-                    if here < half - 1:
-                        chain(y, head).wait_send()
+            def each(head, carry):
+                ask(place, head).wait_send()
+                tell(place, head).wait_send()
                 return carry
 
-            lax.fori_loop(0, heads, drain, 0)
-
-    @pl.when(upper)
-    def _():
-        def drain(head, carry):
-            ask(head).wait_send()
-            tell(head).wait_send()
-            return carry
-
-        lax.fori_loop(0, heads, drain, 0)
-
-    @pl.when(is_middle)
-    def _():
-        def drain(head, carry):
+            lax.fori_loop(0, heads, each, 0)
+
+    def answered():
+        def each(head, carry):
             for i in range(half):
                 answer(i, head).wait_send()
                 answer_total(i, head).wait_send()
             return carry
 
-        lax.fori_loop(0, heads, drain, 0)
+        lax.fori_loop(0, heads, each, 0)
+
+    return drain, answered
 
 
 def grid_of(count):
@@ -379,14 +436,13 @@
     line = lax.broadcasted_iota(jnp.int32, square, 0)
     named = r.routes[...]
     weight = r.route_weight[...]
-    share = weight / jnp.sum(weight, axis=1, keepdims=True)
+    share = weight / jnp.sum(weight, axis=0, keepdims=True)
     chosen = jnp.zeros(square, F32)
     gate = jnp.zeros(square, F32)
     for k in range(TOP):
-        match = named[:, k : k + 1] == lane
+        match = named[k : k + 1] == line
         chosen = chosen + jnp.where(match, 1.0, 0.0)
-        gate = gate + jnp.where(match, share[:, k : k + 1], 0.0)
-    chosen, gate = chosen.T, gate.T
+        gate = gate + jnp.where(match, share[k : k + 1], 0.0)
     earlier = jnp.dot(
         chosen.astype(BF16),
         jnp.where(line < lane, 1.0, 0.0).astype(BF16),
@@ -426,15 +482,23 @@
         )
         copy.start()
         copies.append(copy)
-    summed = piece(me)
-    for at, copy in reversed(list(enumerate(copies))):
-        copy.wait_recv()
-        summed = summed + r.branch_in[at].astype(F32)
-    r.stream[...] = (r.residual[...].astype(F32) + summed).astype(BF16)
-    return copies
-
-
-def experts_part(r, loaded):
+    r.branch_own[...] = r.residual[...].astype(F32) + piece(me)
+
+    def settle():
+        summed = r.branch_own[...]
+        for at, copy in reversed(list(enumerate(copies))):
+            copy.wait_recv()
+            summed = summed + r.branch_in[at].astype(F32)
+        r.stream[...] = summed.astype(BF16)
+
+    def drain():
+        for copy in copies:
+            copy.wait_send()
+
+    return settle, drain
+
+
+def experts_part(r):
     offsets, ny, nx = peer_offsets()
     seq, heads = lax.axis_size("sp"), lax.axis_size("tp")
     me, mine = lax.axis_index("sp"), lax.axis_index("tp")
@@ -446,8 +510,14 @@
     across_x, across_y, across_both = peer_at(0, 1), peer_at(1, 0), peer_at(1, 1)
     top, bottom = pl.ds(0, slots), pl.ds(slots, slots)
 
-    def source(step):
-        return lax.rem(chip + chips - step, chips)
+    half = chips // 2
+
+    def source(k):
+        late = half + lax.rem(lax.rem(chip, half) + 1 + k, half)
+        return jnp.where(k < half, k, late)
+
+    def distance(k):
+        return lax.rem(chip + chips - source(k), chips)
 
     def outgoing(step, side):
         target_core = core if side == 0 else 1 - core
@@ -461,34 +531,36 @@
             expert,
         )
 
-    for step in range(chips):
-        for side in range(2):
-            expert, copy = outgoing(step, side)
-            picked = jnp.dot(r.select[expert], r.stream[...], preferred_element_type=F32)
-            if step == 0 and side == 0:
-                r.rows[chip, block_of(core, slots), block_of(mine, width)] = picked.astype(BF16)
-            else:
-                r.send[expert] = picked.astype(BF16)
-                copy.start()
-
-    def incoming(step, side):
+    def send_out(steps):
+        for step in sorted(steps, key=lambda step: (step == 0, step % 2 == 0, -step)):
+            for side in range(2):
+                expert, copy = outgoing(step, side)
+                picked = jnp.dot(r.select[expert], r.stream[...], preferred_element_type=F32)
+                if step == 0 and side == 0:
+                    place = (chip, block_of(core, slots), block_of(mine, width))
+                    r.rows[place] = picked.astype(BF16)
+                else:
+                    r.send[expert] = picked.astype(BF16)
+                    copy.start()
+
+    def incoming(k, side):
         origin_core = core if side == 0 else 1 - core
-        origin = source(step)
+        origin = source(k)
         return remote(
             r.send.at[me],
             r.rows.at[origin, block_of(origin_core, slots), block_of(mine, width)],
-            r.out_s.at[step, side],
-            r.out_r.at[step, side],
+            r.out_s.at[distance(k), side],
+            r.out_r.at[distance(k), side],
             "sp",
             2 * origin + origin_core,
         )
 
-    def land(step):
-        @pl.when(step > 0)
+    def land(k):
+        @pl.when(distance(k) > 0)
         def _():
-            incoming(step, 0).wait_recv()
-
-        incoming(step, 1).wait_recv()
+            incoming(k, 0).wait_recv()
+
+        incoming(k, 1).wait_recv()
 
     def spread(step, at, peer, owner):
         ref = r.rows.at[source(step), :, block_of(owner, width)]
@@ -590,8 +662,8 @@
         return remote(
             r.summed.at[step, side],
             r.back.at[me],
-            r.home_s.at[step, side],
-            r.home_r.at[step, side],
+            r.home_s.at[distance(step), side],
+            r.home_r.at[distance(step), side],
             "sp",
             2 * source(step) + origin_core,
         )
@@ -635,82 +707,92 @@
         r.summed[step, 0] = r.sums[core]
         r.summed[step, 1] = r.sums[1 - core]
 
-        @pl.when(step == 0)
+        @pl.when(distance(step) == 0)
         def _():
-            r.back[me] = r.summed[0, 0]
-
-        @pl.when(step > 0)
+            r.back[me] = r.summed[step, 0]
+
+        @pl.when(distance(step) > 0)
         def _():
             home(step, 0).start()
 
         home(step, 1).start()
 
-    loaded()
-    start_spread(0)
-    if chips > 1:
-        start_spread(1)
-    start_relay(0)
-
-    def body(step, carry):
-        @pl.when(step + 2 < chips)
-        def _():
-            start_spread(step + 2)
-
-        @pl.when(step + 1 < chips)
-        def _():
-            start_relay(step + 1)
-
-        @pl.when(step < chips)
-        def _():
-            compute(step)
-            start_first(step)
-
-        @pl.when((step >= 1) & (step < chips + 1))
-        def _():
-            start_second(step - 1)
-
-        @pl.when(step >= 2)
-        def _():
-            start_home(step - 2)
-
-        return carry
-
-    lax.fori_loop(0, chips + 2, body, 0)
-
-    def arrive(step, carry):
-        @pl.when(step > 0)
-        def _():
-            returned(step, 0).wait_recv()
-
-        returned(step, 1).wait_recv()
-        return carry
-
-    lax.fori_loop(0, chips, arrive, 0)
-    back = r.back[...].reshape(experts * slots, width)
-    mixed = jnp.dot(r.high[...], back, preferred_element_type=F32)
-    mixed = mixed + jnp.dot(r.low[...], back, preferred_element_type=F32)
-    r.out[...] = (r.stream[...].astype(F32) + mixed).astype(BF16)
-
-    def drain(step, carry):
-        @pl.when(step > 0)
-        def _():
-            outgoing(step, 0)[1].wait_send()
-            home(step, 0).wait_send()
-
-        outgoing(step, 1)[1].wait_send()
-        home(step, 1).wait_send()
-        for at, offset in enumerate(near):
-            spread(step, at, peer_at(*offset), mine).wait_send()
-        if square:
-            relay(step, 0, across_y, across_x).wait_send()
-            relay(step, 1, across_x, across_y).wait_send()
-            for copy in second_copies(step):
+    def start():
+        start_spread(0)
+
+    def first_relay():
+        start_relay(0)
+
+    def others():
+        def body(k, carry):
+            @pl.when(k < chips)
+            def _():
+                start_relay(k)
+
+            @pl.when(k + 1 < chips)
+            def _():
+                start_spread(k + 1)
+
+            @pl.when(k < chips)
+            def _():
+                compute(k)
+                start_first(k)
+
+            @pl.when(k < chips + 1)
+            def _():
+                start_second(k - 1)
+
+            @pl.when(k >= 2)
+            def _():
+                start_home(k - 2)
+
+            return carry
+
+        lax.fori_loop(1, chips + 2, body, 0)
+        finish()
+
+    def finish():
+        def arrive(step, carry):
+            @pl.when(step > 0)
+            def _():
+                returned(step, 0).wait_recv()
+
+            returned(step, 1).wait_recv()
+            return carry
+
+        lax.fori_loop(0, chips, arrive, 0)
+        back = r.back[...].reshape(experts * slots, width)
+        mixed = jnp.dot(r.high[...], back, preferred_element_type=F32)
+        mixed = mixed + jnp.dot(r.low[...], back, preferred_element_type=F32)
+        r.out[...] = (r.stream[...].astype(F32) + mixed).astype(BF16)
+
+    def drain():
+        def each(k, carry):
+            @pl.when(k > 0)
+            def _():
+                outgoing(k, 0)[1].wait_send()
+
+            outgoing(k, 1)[1].wait_send()
+
+            @pl.when(distance(k) > 0)
+            def _():
+                home(k, 0).wait_send()
+
+            home(k, 1).wait_send()
+            for at, offset in enumerate(near):
+                spread(k, at, peer_at(*offset), mine).wait_send()
+            if square:
+                relay(k, 0, across_y, across_x).wait_send()
+                relay(k, 1, across_x, across_y).wait_send()
+                for copy in second_copies(k):
+                    copy.wait_send()
+            for copy in first_copies(k):
                 copy.wait_send()
-        for copy in first_copies(step):
-            copy.wait_send()
-        return carry
-
-    lax.fori_loop(0, chips, drain, 0)
+            return carry
+
+        lax.fori_loop(0, chips, each, 0)
+
+    return send_out, start, first_relay, compute, start_first, start_spread, others, drain
 
 
 def layer(args):
@@ -730,7 +812,7 @@
     first_shape = (4, slots, width) if square else (heads_dev - 1, 2 * slots, width)
     dma = pltpu.SemaphoreType.DMA
     big = ("qa", "ka", "va", "qb", "kb", "vb", "residual", "proj_a", "proj_b", "gate", "up", "down")
-    small = ("lam", "gain_a", "gain_b", "norm_gain", "routes", "route_weight")
+    small = ("lam_a", "lam_b", "gain_a", "gain_b", "norm_gain", "routes", "route_weight")
 
     def landing(name):
         shape = args[name].shape
@@ -743,6 +825,7 @@
     scratch = {name: landing(name) for name in big}
     scratch.update(
         load_s=dma((len(big),)),
+        go=pltpu.SemaphoreType.REGULAR,
         heads_a=pltpu.VMEM((rows, heads * value_a), BF16),
         heads_b=pltpu.VMEM((rows, heads * value_b), BF16),
         kv=pltpu.VMEM((blocks, heads, rows, width_a + value_a + width_b + value_b), BF16),
@@ -755,13 +838,14 @@
         far_part=pltpu.VMEM((heads, rows, value_a + value_b), BF16),
         total=pltpu.VMEM((half, heads, 8, rows), F32),
         far_total=pltpu.VMEM((heads, 8, rows), F32),
-        chain_s=dma((half, heads)), chain_r=dma((half, heads)),
-        part_s=dma((half, heads)), part_r=dma((half, heads)),
+        chain_s=dma((half, heads, 2)), chain_r=dma((half, heads, 2)),
+        part_s=dma((half, heads, 2)), part_r=dma((half, heads, 2)),
         query_s=dma((heads,)), query_r=dma((half, heads)),
         stats_s=dma((heads,)), stats_r=dma((half, heads)),
         back_s=dma((half, heads)), back_r=dma((heads,)),
         total_s=dma((half, heads)), total_r=dma((heads,)),
         branch_out=pltpu.VMEM((heads_dev - 1, rows, width), BF16),
+        branch_own=pltpu.VMEM((rows, width), F32),
         branch_in=pltpu.VMEM((heads_dev - 1, rows, width), BF16),
         branch_s=dma((heads_dev - 1,)), branch_r=dma((heads_dev - 1,)),
         stream=pltpu.VMEM((rows, width), BF16),
@@ -808,16 +892,56 @@
 
         for name in big:
             load(name).start()
-        greet(("sp", "tp"))
-        attend(r, lambda: wait("qa", "ka", "va", "qb", "kb", "vb"))
-        route(r)
-        copies = project(r, lambda: wait("residual", "proj_a", "proj_b"))
-        experts_part(r, lambda: wait("gate", "up", "down"))
-        for copy in copies:
-            copy.wait_send()
+        greeted = greet(("sp", "tp"))
+        (
+            send_out, start, first_relay, compute, start_first, start_spread, others, drain_experts,
+        ) = experts_part(r)
+        chip = lax.axis_index("sp") // 2
+        drain_heads, answered = attend(
+            r, lambda: wait("qa", "ka", "va", "qb", "kb", "vb"), greeted, lambda: route(r)
+        )
+
+        settle, drain_branch = project(r, lambda: wait("residual", "proj_a", "proj_b"))
+        wait("gate", "up", "down")
+
+        @pl.when(chip == half - 1)
+        def _():
+            answered()
+            if half > 1:
+                pl.semaphore_signal(
+                    r.go, inc=1, device_id={"sp": lax.rem(lax.axis_index("sp"), 2)}, device_id_type=MESH
+                )
+
+        @pl.when(chip == 0)
+        def _():
+            settle()
+            send_out(range(half))
+            start()
+            first_relay()
+            compute(0)
+            start_first(0)
+            if half > 1:
+                pl.semaphore_wait(r.go, 1)
+            send_out(range(half, chips))
+            start_spread(1)
+
+        @pl.when(chip > 0)
+        def _():
+            start()
+            settle()
+            send_out(range(chips))
+            first_relay()
+            start_spread(1)
+            compute(0)
+            start_first(0)
+
+        others()
+        drain_heads()
+        drain_branch()
+        drain_experts()
 
     vmem = pl.BlockSpec(memory_space=pltpu.VMEM)
-    specs = [pl.BlockSpec(memory_space=pltpu.SMEM)] + [vmem] * (len(small) - 1)
+    specs = [pl.BlockSpec(memory_space=pltpu.SMEM)] * 2 + [vmem] * (len(small) - 2)
     specs += [pl.BlockSpec(memory_space=pl.ANY)] * len(big)
     return pl.pallas_call(
         kernel,
@@ -861,14 +985,15 @@
         qb=query_b,
         kb=keys_b,
         vb=values_b,
-        lam=jnp.stack([lambda_a, lambda_b]),
+        lam_a=lambda_a,
+        lam_b=lambda_b,
         gain_a=gain_a.reshape(1, -1),
         gain_b=gain_b.reshape(1, -1),
         proj_a=proj_a,
         proj_b=proj_b,
         norm_gain=norm_gain.reshape(1, -1),
-        routes=routes,
-        route_weight=route_weight,
+        routes=routes.T,
+        route_weight=route_weight.T,
         gate=expert_gate,
         up=expert_up,
         down=expert_down,

time: 117 us -> 97.6 us (0.83)
  the two profiles are of different devices: /device:TPU:0 before, /device:TPU:25 now
where the time goes in v3:
time: 97.6 us; the launch traced here: 97.4 us
  Pallas kernels  95.8 us (98%)
  local copies, waits for them, and re-layouts  1.57 us (2%)
    pallas_call x1, Pallas kernels, layer(): pl.pallas_call(kernel, out_shape=jax.ShapeDtypeStruct((rows, width), BF16...  95.8 us

profile of v3, /device:TPU:25, one launch (start us, length us, event | category | flops | bytes accessed | tf_op | source)
XLA Modules:
  0.0 97.4 jit_solution(1329853916767423388)
XLA Ops:
  0.0 95.8 %layer.1 = bf16[128,512]{1,0:T(8,128)(2,1)} custom-call(f32[4]{0:T(128)} %refs_0_.1, f32[4]{0:T(128)} %refs_1_.1, f32[1,128]{1,0:T(1,128)} %bitcast.9, f32[1,256]{1,0:T(1,128)} %bitcast.6, f32[1,2048]{1,0:T(1,128)} %bitcast.5, s32[2,128]{1,0:T(2,128)} %bitcast.7, f32[2,128]{1,0:T(2,128)} %bitcast.8, bf16[128,4,128]{2,1,0:T(4,128)(2,1)} %refs_7_.1, ...), custom_call_target="tpu_custom_call" | custom-call | tf_op jit(solution)/shard_map/layer/pallas_call | solution.py:946
  95.8 1.6 %copy.21 = bf16[128,512]{1,0:T(8,128)(2,1)} copy(bf16[128,512]{1,0:T(8,128)(2,1)} %layer.1) | data formatting | bytes 262144

commit v4 on v3

--- a/solution.py
+++ b/solution.py
@@ -130,15 +130,18 @@
             "sp", 2 * (half + i) + core,
         )
 
-    def pack(head):
+    def pack_keys(head):
         query[head, :, :width_a] = r.qa[:, head, :]
         query[head, :, width_a:] = r.qb[:, head, :]
-        for span, ref in zip(key_spans + value_spans, (r.ka, r.kb, r.va, r.vb)):
+        for span, ref in zip(key_spans, (r.ka, r.kb)):
             kv[slot, head, :, span[0] : span[0] + span[1]] = ref[:, head, :]
 
+    def pack_values(head):
+        for span, ref in zip(value_spans, (r.va, r.vb)):
+            kv[slot, head, :, span[0] : span[0] + span[1]] = ref[:, head, :]
+
     arrived()
-    for head in range(heads):
-        pack(head)
+    pack_keys(0)
     greeted()
 
     def give(head, part):
@@ -150,17 +153,22 @@
 
     @pl.when(upper)
     def _():
+        ask(place, 0).start()
         for head in range(heads):
-            if head == 0:
-                ask(place, head).start()
+            if head:
+                pack_keys(head)
             give(head, 0)
         for head in range(heads):
+            pack_values(head)
             give(head, 1)
 
     @pl.when(lower)
     def _():
         for head in range(heads):
+            if head:
+                pack_keys(head)
             give(head, 0)
+            pack_values(head)
             give(head, 1)
 
     def pass_on(here, head, part):
@@ -237,7 +245,7 @@
         for at in range(pair):
             tell(i + at, head).wait_recv()
 
-    def for_upper(i, head):
+    def for_upper(i, head, values_here):
         queries = r.far_query[pl.ds(i, pair), head].reshape(pair * rows, wide_q)
         maps = score_maps(queries, head, blocks)
         far = jnp.concatenate(
@@ -254,6 +262,7 @@
             stats.append((top, summed))
             expos.append(expo)
             scales.append(down / summed)
+        values_here()
         for group in range(2):
             first = expos[2 * group] * scales[2 * group]
             second = expos[2 * group + 1] * (lams[group][head] * scales[2 * group + 1])
@@ -310,24 +319,26 @@
             meanwhile()
 
             pass_on(here, 0, 0)
-            pass_on(here, 0, 1)
+
+            def values_here(head):
+                landed(here, head, 1)
 
             def step(head, carry):
                 landed(here, head, 0)
-                landed(here, head, 1)
+                pl.when(head == 0)(lambda: pass_on(here, 0, 1))
+                if here < half - 1:
+                    values_here(head)
                 if here == half - 1:
 
                     def each(i, inner):
                         wait_far(i * pair, head)
-                        for_upper(i * pair, head)
+                        for_upper(i * pair, head, lambda: None)
                         return inner
 
+                    wait_far(0, head)
+                    for_upper(0, head, lambda: values_here(head))
                     lax.fori_loop(1, half // pair, each, 0)
-                    wait_far(0, head)
-                    own_lower(head, 2 * here + 2)
-                    for_upper(0, head)
-                else:
-                    own_lower(head, 2 * here + 2)
+                own_lower(head, 2 * here + 2)
                 if here:
 
                     @pl.when((head == 0) & (heads > 1))
@@ -349,6 +360,8 @@
             def step(head, carry):
                 gather(here, head, 0)
                 upper_first(head, 2 * here + 2)
+                if here < half - 1:
+                    chain(here, head, 0).wait_send()
 
                 @pl.when(head + 1 < heads)
                 def _():
@@ -381,7 +394,10 @@
                         for part in range(2):
                             across(y, head, part).wait_send()
                             if here < half - 1:
-                                chain(y, head, part).wait_send()
+                                if y == here and part == 0:
+                                    pl.when(lower)(chain(y, head, part).wait_send)
+                                else:
+                                    chain(y, head, part).wait_send()
                     return carry
 
                 lax.fori_loop(0, heads, each, 0)
@@ -585,10 +601,12 @@
             relay(step, 0, across_y, across_x).start()
             relay(step, 1, across_x, across_y).start()
 
-    def compute(step):
+    def ready(step):
         if square:
             relay(step, 0, across_y, across_both).wait_recv()
             relay(step, 1, across_x, across_both).wait_recv()
+
+    def compute(step):
         origin = source(step)
         wide = r.rows[origin].astype(F32)
         mean_sq = jnp.mean(wide * wide, axis=1, keepdims=True)
@@ -725,30 +743,27 @@
 
     def others():
         def body(k, carry):
-            @pl.when(k < chips)
-            def _():
-                start_relay(k)
+            start_relay(k)
 
             @pl.when(k + 1 < chips)
             def _():
                 start_spread(k + 1)
 
-            @pl.when(k < chips)
-            def _():
-                compute(k)
-                start_first(k)
-
-            @pl.when(k < chips + 1)
-            def _():
-                start_second(k - 1)
+            ready(k)
+            start_second(k - 1)
 
             @pl.when(k >= 2)
             def _():
                 start_home(k - 2)
 
+            compute(k)
+            start_first(k)
             return carry
 
-        lax.fori_loop(1, chips + 2, body, 0)
+        lax.fori_loop(1, chips, body, 0)
+        start_home(chips - 2)
+        start_second(chips - 1)
+        start_home(chips - 1)
         finish()
 
     def finish():
@@ -792,7 +807,7 @@
 
         lax.fori_loop(0, chips, each, 0)
 
-    return send_out, start, first_relay, compute, start_first, start_spread, others, drain
+    return send_out, start, first_relay, ready, compute, start_first, start_spread, others, drain
 
 
 def layer(args):
@@ -894,7 +909,8 @@
             load(name).start()
         greeted = greet(("sp", "tp"))
         (
-            send_out, start, first_relay, compute, start_first, start_spread, others, drain_experts,
+            send_out, start, first_relay, ready, compute, start_first, start_spread, others,
+            drain_experts,
         ) = experts_part(r)
         chip = lax.axis_index("sp") // 2
         drain_heads, answered = attend(
@@ -918,6 +934,7 @@
             send_out(range(half))
             start()
             first_relay()
+            ready(0)
             compute(0)
             start_first(0)
             if half > 1:
@@ -932,6 +949,7 @@
             send_out(range(chips))
             first_relay()
             start_spread(1)
+            ready(0)
             compute(0)
             start_first(0)
 

time: 97.6 us -> 91.4 us (0.936)
  Pallas kernels: 95.8 us -> 89.6 us
    pallas_call x1, Pallas kernels: 95.8 us -> 89.6 us  [layer(): pl.pallas_call(kernel, out_shape=jax.ShapeDtypeStruct((rows, width), BF16...]
where the time goes in v4:
time: 91.4 us; the launch traced here: 91.2 us
  Pallas kernels  89.6 us (98%)
  local copies, waits for them, and re-layouts  1.57 us (2%)
    pallas_call x1, Pallas kernels, layer(): pl.pallas_call(kernel, out_shape=jax.ShapeDtypeStruct((rows, width), BF16...  89.6 us

profile of v4, /device:TPU:25, one launch (start us, length us, event | category | flops | bytes accessed | tf_op | source)
XLA Modules:
  0.0 91.2 jit_solution(15789894468054481643)
XLA Ops:
  0.0 89.6 %layer.1 = bf16[128,512]{1,0:T(8,128)(2,1)} custom-call(f32[4]{0:T(128)} %refs_0_.1, f32[4]{0:T(128)} %refs_1_.1, f32[1,128]{1,0:T(1,128)} %bitcast.9, f32[1,256]{1,0:T(1,128)} %bitcast.6, f32[1,2048]{1,0:T(1,128)} %bitcast.5, s32[2,128]{1,0:T(2,128)} %bitcast.7, f32[2,128]{1,0:T(2,128)} %bitcast.8, bf16[128,4,128]{2,1,0:T(4,128)(2,1)} %refs_7_.1, ...), custom_call_target="tpu_custom_call" | custom-call | tf_op jit(solution)/shard_map/layer/pallas_call | solution.py:964
  89.6 1.6 %copy.21 = bf16[128,512]{1,0:T(8,128)(2,1)} copy(bf16[128,512]{1,0:T(8,128)(2,1)} %layer.1) | data formatting | bytes 262144

commit v5 on v4

--- a/solution.py
+++ b/solution.py
@@ -30,6 +30,10 @@
         device_id={axis: peer},
         device_id_type=MESH,
     )
+
+
+def wait_bytes(ref, semaphore):
+    pltpu.make_async_copy(ref, ref, semaphore).wait()
 
 
 def greet(axes):
@@ -103,30 +107,30 @@
     def across(y, head, part):
         ref = kv.at[2 * y + core, head, :, parts_of[part]]
         return remote(
-            ref, ref, r.part_s.at[y, head, part], r.part_r.at[y, head, part], "sp", partner
+            ref, ref, r.part_s.at[0], r.part_r.at[head, part], "sp", partner
         )
 
     def ask(i, head):
         return remote(
-            query.at[head], r.far_query.at[i, head], r.query_s.at[head], r.query_r.at[i, head],
+            query.at[head], r.far_query.at[i, head], r.query_s.at[0], r.query_r.at[i, head],
             "sp", middle,
         )
 
     def tell(i, head):
         return remote(
-            r.own_stats.at[head], r.far_stats.at[i, head], r.stats_s.at[head],
+            r.own_stats.at[head], r.far_stats.at[i, head], r.stats_s.at[0],
             r.stats_r.at[i, head], "sp", middle,
         )
 
     def answer(i, head):
         return remote(
-            r.part.at[i, head], r.far_part.at[head], r.back_s.at[i, head], r.back_r.at[head],
+            r.part.at[i, head], r.far_part.at[head], r.back_s.at[0], r.back_r.at[head],
             "sp", 2 * (half + i) + core,
         )
 
     def answer_total(i, head):
         return remote(
-            r.total.at[i, head], r.far_total.at[head], r.total_s.at[i, head], r.total_r.at[head],
+            r.total.at[i, head], r.far_total.at[head], r.total_s.at[0], r.total_r.at[head],
             "sp", 2 * (half + i) + core,
         )
 
@@ -179,8 +183,7 @@
                 chain(y, head, part).start()
 
     def landed(here, head, part):
-        for y in range(here + 1):
-            across(y, head, part).wait_recv()
+        wait_bytes(kv.at[: here + 1, head, :, parts_of[part]], r.part_r.at[head, part])
 
     def gather(here, head, part):
         pass_on(here, head, part)
@@ -389,36 +392,28 @@
 
             @pl.when(place == here)
             def _():
-                def each(head, carry):
-                    for y in range(here + 1):
-                        for part in range(2):
-                            across(y, head, part).wait_send()
-                            if here < half - 1:
-                                if y == here and part == 0:
-                                    pl.when(lower)(chain(y, head, part).wait_send)
-                                else:
-                                    chain(y, head, part).wait_send()
-                    return carry
-
-                lax.fori_loop(0, heads, each, 0)
+                wait_bytes(kv.at[: here + 1], r.part_s.at[0])
+                if here < half - 1:
+
+                    def each(head, carry):
+                        for y in range(here + 1):
+                            if y < here:
+                                chain(y, head, 0).wait_send()
+                            else:
+                                pl.when(lower)(chain(y, head, 0).wait_send)
+                            chain(y, head, 1).wait_send()
+                        return carry
+
+                    lax.fori_loop(0, heads, each, 0)
 
         @pl.when(upper)
         def _():
-            def each(head, carry):
-                ask(place, head).wait_send()
-                tell(place, head).wait_send()
-                return carry
-
-            lax.fori_loop(0, heads, each, 0)
+            wait_bytes(query, r.query_s.at[0])
+            wait_bytes(r.own_stats, r.stats_s.at[0])
 
     def answered():
-        def each(head, carry):
-            for i in range(half):
-                answer(i, head).wait_send()
-                answer_total(i, head).wait_send()
-            return carry
-
-        lax.fori_loop(0, heads, each, 0)
+        wait_bytes(r.part, r.back_s.at[0])
+        wait_bytes(r.total, r.total_s.at[0])
 
     return drain, answered
 
@@ -494,7 +489,7 @@
         peer = peer_at(*offset)
         r.branch_out[at] = piece(peer).astype(BF16)
         copy = remote(
-            r.branch_out.at[at], r.branch_in.at[at], r.branch_s.at[at], r.branch_r.at[at], "tp", peer
+            r.branch_out.at[at], r.branch_in.at[at], r.branch_s.at[0], r.branch_r.at[at], "tp", peer
         )
         copy.start()
         copies.append(copy)
@@ -508,8 +503,7 @@
         r.stream[...] = summed.astype(BF16)
 
     def drain():
-        for copy in copies:
-            copy.wait_send()
+        wait_bytes(r.branch_out, r.branch_s.at[0])
 
     return settle, drain
 
@@ -541,8 +535,8 @@
         return expert, remote(
             r.send.at[expert],
             r.rows.at[chip, block_of(core, slots), block_of(mine, width)],
-            r.out_s.at[step, side],
-            r.out_r.at[step, side],
+            r.out_s.at[0],
+            r.out_r.at[step],
             "sp",
             expert,
         )
@@ -559,32 +553,22 @@
                     r.send[expert] = picked.astype(BF16)
                     copy.start()
 
-    def incoming(k, side):
-        origin_core = core if side == 0 else 1 - core
-        origin = source(k)
-        return remote(
-            r.send.at[me],
-            r.rows.at[origin, block_of(origin_core, slots), block_of(mine, width)],
-            r.out_s.at[distance(k), side],
-            r.out_r.at[distance(k), side],
-            "sp",
-            2 * origin + origin_core,
-        )
-
     def land(k):
         @pl.when(distance(k) > 0)
         def _():
-            incoming(k, 0).wait_recv()
-
-        incoming(k, 1).wait_recv()
+            wait_bytes(r.rows.at[source(k), :, block_of(mine, width)], r.out_r.at[distance(k)])
+
+        @pl.when(distance(k) == 0)
+        def _():
+            wait_bytes(r.rows.at[source(k), bottom, block_of(mine, width)], r.out_r.at[0])
 
     def spread(step, at, peer, owner):
         ref = r.rows.at[source(step), :, block_of(owner, width)]
-        return remote(ref, ref, r.spread_s.at[step, at], r.spread_r.at[step, at], "tp", peer)
+        return remote(ref, ref, r.spread_s.at[0], r.spread_r.at[step], "tp", peer)
 
     def relay(step, at, peer, owner):
         ref = r.rows.at[source(step), top if at == 0 else bottom, block_of(owner, width)]
-        return remote(ref, ref, r.relay_s.at[step, at], r.relay_r.at[step, at], "tp", peer)
+        return remote(ref, ref, r.relay_s.at[0], r.relay_r.at[step], "tp", peer)
 
     near = ((0, 1), (1, 0)) if square else offsets
 
@@ -594,17 +578,14 @@
             spread(step, at, peer_at(*offset), mine).start()
 
     def start_relay(step):
-        for at, offset in enumerate(near):
-            giver = peer_at(ny - offset[0], nx - offset[1])
-            spread(step, at, giver, giver).wait_recv()
+        wait_bytes(r.rows.at[source(step), :, : len(near) * width], r.spread_r.at[step])
         if square:
             relay(step, 0, across_y, across_x).start()
             relay(step, 1, across_x, across_y).start()
 
     def ready(step):
         if square:
-            relay(step, 0, across_y, across_both).wait_recv()
-            relay(step, 1, across_x, across_both).wait_recv()
+            wait_bytes(r.rows.at[source(step), :, :width], r.relay_r.at[step])
 
     def compute(step):
         origin = source(step)
@@ -622,8 +603,8 @@
                 remote(
                     r.down_out.at[step, :, block_of(peer_at(*offset), width)],
                     r.first.at[step, at],
-                    r.first_s.at[step, at],
-                    r.first_r.at[step, at],
+                    r.first_s.at[0],
+                    r.first_r.at[step, 0],
                     "tp",
                     peer_at(*offset),
                 )
@@ -639,8 +620,8 @@
             remote(
                 r.down_out.at[step, part, block_of(owner, width)],
                 r.first.at[step, slot],
-                r.first_s.at[step, slot],
-                r.first_r.at[step, slot],
+                r.first_s.at[0],
+                r.first_r.at[step, slot % 2],
                 "tp",
                 peer,
             )
@@ -652,8 +633,8 @@
             remote(
                 r.second_out.at[step, at],
                 r.second.at[step, at],
-                r.second_s.at[step, at],
-                r.second_r.at[step, at],
+                r.second_s.at[0],
+                r.second_r.at[step],
                 "tp",
                 peer,
             )
@@ -667,9 +648,9 @@
     def start_second(step):
         if not square:
             return
-        firsts, seconds = first_copies(step), second_copies(step)
+        seconds = second_copies(step)
+        wait_bytes(r.first.at[step, :2], r.first_r.at[step, 1])
         for at, part, owner, slot in ((0, top, across_y, 1), (1, bottom, across_x, 3)):
-            firsts[at].wait_recv()
             summed = r.down_out[step, part, block_of(owner, width)].astype(F32)
             summed = summed + r.first[step, slot].astype(F32)
             r.second_out[step, at] = summed.astype(BF16)
@@ -680,34 +661,19 @@
         return remote(
             r.summed.at[step, side],
             r.back.at[me],
-            r.home_s.at[distance(step), side],
-            r.home_r.at[distance(step), side],
+            r.home_s.at[0],
+            r.home_r.at[0],
             "sp",
             2 * source(step) + origin_core,
         )
 
-    def returned(step, side):
-        expert_core = core if side == 0 else 1 - core
-        expert = 2 * lax.rem(chip + step, chips) + expert_core
-        return remote(
-            r.summed.at[step, side],
-            r.back.at[expert],
-            r.home_s.at[step, side],
-            r.home_r.at[step, side],
-            "sp",
-            expert,
-        )
-
     def start_home(step):
         own = block_of(mine, width)
-        firsts = first_copies(step)
         if square:
-            seconds = second_copies(step)
-            firsts[2].wait_recv()
-            firsts[3].wait_recv()
+            wait_bytes(r.first.at[step, :2], r.first_r.at[step, 0])
+            wait_bytes(r.second.at[step], r.second_r.at[step])
             halves = []
             for at, part, slot in ((0, top, 0), (1, bottom, 2)):
-                seconds[at].wait_recv()
                 halves.append(
                     r.down_out[step, part, own].astype(F32)
                     + r.first[step, slot].astype(F32)
@@ -716,9 +682,9 @@
             r.sums[0] = halves[0].astype(BF16)
             r.sums[1] = halves[1].astype(BF16)
         else:
+            wait_bytes(r.first.at[step], r.first_r.at[step, 0])
             summed = r.down_out[step, :, own].astype(F32)
-            for at, copy in enumerate(firsts):
-                copy.wait_recv()
+            for at in range(len(offsets)):
                 summed = summed + r.first[step, at].astype(F32)
             r.sums[0] = summed[:slots].astype(BF16)
             r.sums[1] = summed[slots:].astype(BF16)
@@ -767,45 +733,20 @@
         finish()
 
     def finish():
-        def arrive(step, carry):
-            @pl.when(step > 0)
-            def _():
-                returned(step, 0).wait_recv()
-
-            returned(step, 1).wait_recv()
-            return carry
-
-        lax.fori_loop(0, chips, arrive, 0)
+        wait_bytes(r.back.at[: experts - 1], r.home_r.at[0])
         back = r.back[...].reshape(experts * slots, width)
         mixed = jnp.dot(r.high[...], back, preferred_element_type=F32)
         mixed = mixed + jnp.dot(r.low[...], back, preferred_element_type=F32)
         r.out[...] = (r.stream[...].astype(F32) + mixed).astype(BF16)
 
     def drain():
-        def each(k, carry):
-            @pl.when(k > 0)
-            def _():
-                outgoing(k, 0)[1].wait_send()
-
-            outgoing(k, 1)[1].wait_send()
-
-            @pl.when(distance(k) > 0)
-            def _():
-                home(k, 0).wait_send()
-
-            home(k, 1).wait_send()
-            for at, offset in enumerate(near):
-                spread(k, at, peer_at(*offset), mine).wait_send()
-            if square:
-                relay(k, 0, across_y, across_x).wait_send()
-                relay(k, 1, across_x, across_y).wait_send()
-                for copy in second_copies(k):
-                    copy.wait_send()
-            for copy in first_copies(k):
-                copy.wait_send()
-            return carry
-
-        lax.fori_loop(0, chips, each, 0)
+        wait_bytes(r.send.at[: experts - 1], r.out_s.at[0])
+        wait_bytes(r.back.at[: experts - 1], r.home_s.at[0])
+        wait_bytes(r.rows.at[:, :, : len(near) * width], r.spread_s.at[0])
+        wait_bytes(r.first, r.first_s.at[0])
+        if square:
+            wait_bytes(r.rows.at[:, :, :width], r.relay_s.at[0])
+            wait_bytes(r.second, r.second_s.at[0])
 
     return send_out, start, first_relay, ready, compute, start_first, start_spread, others, drain
 
@@ -823,7 +764,6 @@
     slots = 2 * rows * TOP // seq
     _, ny, nx = peer_offsets()
     square = ny == 2 and nx == 2
-    spreads = 2 if square else heads_dev - 1
     first_shape = (4, slots, width) if square else (heads_dev - 1, 2 * slots, width)
     dma = pltpu.SemaphoreType.DMA
     big = ("qa", "ka", "va", "qb", "kb", "vb", "residual", "proj_a", "proj_b", "gate", "up", "down")
@@ -853,16 +793,16 @@
         far_part=pltpu.VMEM((heads, rows, value_a + value_b), BF16),
         total=pltpu.VMEM((half, heads, 8, rows), F32),
         far_total=pltpu.VMEM((heads, 8, rows), F32),
-        chain_s=dma((half, heads, 2)), chain_r=dma((half, heads, 2)),
-        part_s=dma((half, heads, 2)), part_r=dma((half, heads, 2)),
-        query_s=dma((heads,)), query_r=dma((half, heads)),
-        stats_s=dma((heads,)), stats_r=dma((half, heads)),
-        back_s=dma((half, heads)), back_r=dma((heads,)),
-        total_s=dma((half, heads)), total_r=dma((heads,)),
+        chain_s=dma((max(half - 1, 1), heads, 2)), chain_r=dma((max(half - 1, 1), heads, 2)),
+        part_s=dma((1,)), part_r=dma((heads, 2)),
+        query_s=dma((1,)), query_r=dma((half, heads)),
+        stats_s=dma((1,)), stats_r=dma((half, heads)),
+        back_s=dma((1,)), back_r=dma((heads,)),
+        total_s=dma((1,)), total_r=dma((heads,)),
         branch_out=pltpu.VMEM((heads_dev - 1, rows, width), BF16),
         branch_own=pltpu.VMEM((rows, width), F32),
         branch_in=pltpu.VMEM((heads_dev - 1, rows, width), BF16),
-        branch_s=dma((heads_dev - 1,)), branch_r=dma((heads_dev - 1,)),
+        branch_s=dma((1,)), branch_r=dma((heads_dev - 1,)),
         stream=pltpu.VMEM((rows, width), BF16),
         select=pltpu.VMEM((seq, slots, rows), BF16),
         weigh=pltpu.VMEM((seq * slots, rows), F32),
@@ -870,19 +810,19 @@
         low=pltpu.VMEM((rows, seq * slots), BF16),
         send=pltpu.VMEM((seq, slots, width), BF16),
         rows=pltpu.VMEM((chips, 2 * slots, model), BF16),
-        out_s=dma((chips, 2)), out_r=dma((chips, 2)),
-        spread_s=dma((chips, spreads)), spread_r=dma((chips, spreads)),
-        relay_s=dma((chips, 2)), relay_r=dma((chips, 2)),
+        out_s=dma((1,)), out_r=dma((chips,)),
+        spread_s=dma((1,)), spread_r=dma((chips,)),
+        relay_s=dma((1,)), relay_r=dma((chips,)),
         down_out=pltpu.VMEM((chips, 2 * slots, model), BF16),
         first=pltpu.VMEM((chips,) + first_shape, BF16),
-        first_s=dma((chips, first_shape[0])), first_r=dma((chips, first_shape[0])),
+        first_s=dma((1,)), first_r=dma((chips, 2)),
         second_out=pltpu.VMEM((chips, 2, slots, width), BF16),
         second=pltpu.VMEM((chips, 2, slots, width), BF16),
-        second_s=dma((chips, 2)), second_r=dma((chips, 2)),
+        second_s=dma((1,)), second_r=dma((chips,)),
         sums=pltpu.VMEM((2, slots, width), BF16),
         summed=pltpu.VMEM((chips, 2, slots, width), BF16),
         back=pltpu.VMEM((seq, slots, width), BF16),
-        home_s=dma((chips, 2)), home_r=dma((chips, 2)),
+        home_s=dma((1,)), home_r=dma((1,)),
     )
 
     def kernel(*refs):

time: 91.4 us -> 89.9 us (0.984)
  Pallas kernels: 89.6 us -> 88.2 us
    pallas_call x1, Pallas kernels: 89.6 us -> 88.2 us  [layer(): pl.pallas_call(kernel, out_shape=jax.ShapeDtypeStruct((rows, width), BF16...]
where the time goes in v5:
time: 89.9 us; the launch traced here: 89.8 us
  Pallas kernels  88.2 us (98%)
  local copies, waits for them, and re-layouts  1.57 us (2%)
    pallas_call x1, Pallas kernels, layer(): pl.pallas_call(kernel, out_shape=jax.ShapeDtypeStruct((rows, width), BF16...  88.2 us

profile of v5, /device:TPU:25, one launch (start us, length us, event | category | flops | bytes accessed | tf_op | source)
XLA Modules:
  0.0 89.8 jit_solution(15599427675873478066)
XLA Ops:
  0.0 88.2 %layer.1 = bf16[128,512]{1,0:T(8,128)(2,1)} custom-call(f32[4]{0:T(128)} %refs_0_.1, f32[4]{0:T(128)} %refs_1_.1, f32[1,128]{1,0:T(1,128)} %bitcast.9, f32[1,256]{1,0:T(1,128)} %bitcast.6, f32[1,2048]{1,0:T(1,128)} %bitcast.5, s32[2,128]{1,0:T(2,128)} %bitcast.7, f32[2,128]{1,0:T(2,128)} %bitcast.8, bf16[128,4,128]{2,1,0:T(4,128)(2,1)} %refs_7_.1, ...), custom_call_target="tpu_custom_call" | custom-call | tf_op jit(solution)/shard_map/layer/pallas_call | solution.py:904
  88.2 1.6 %copy.21 = bf16[128,512]{1,0:T(8,128)(2,1)} copy(bf16[128,512]{1,0:T(8,128)(2,1)} %layer.1) | data formatting | bytes 262144

commit v6 on v5

--- a/solution.py
+++ b/solution.py
@@ -541,8 +541,10 @@
             expert,
         )
 
-    def send_out(steps):
-        for step in sorted(steps, key=lambda step: (step == 0, step % 2 == 0, -step)):
+    def send_out(steps, upward=False):
+        for step in sorted(
+            steps, key=lambda step: (step == 0, step if upward else 0, step % 2 == 0, -step)
+        ):
             for side in range(2):
                 expert, copy = outgoing(step, side)
                 picked = jnp.dot(r.select[expert], r.stream[...], preferred_element_type=F32)
@@ -886,7 +888,8 @@
         def _():
             start()
             settle()
-            send_out(range(chips))
+            pl.when(chip >= half)(lambda: send_out(range(chips)))
+            pl.when(chip < half)(lambda: send_out(range(chips), True))
             first_relay()
             start_spread(1)
             ready(0)

time: 89.9 us -> 89.6 us (level)
  no operation moved by 1% of the time
where the time goes in v6:
time: 89.6 us; the launch traced here: 89.4 us
  Pallas kernels  87.8 us (98%)
  local copies, waits for them, and re-layouts  1.57 us (2%)
    pallas_call x1, Pallas kernels, layer(): pl.pallas_call(kernel, out_shape=jax.ShapeDtypeStruct((rows, width), BF16...  87.8 us

profile of v6, /device:TPU:25, one launch (start us, length us, event | category | flops | bytes accessed | tf_op | source)
XLA Modules:
  0.0 89.4 jit_solution(12773493473812142820)
XLA Ops:
  0.0 87.8 %layer.1 = bf16[128,512]{1,0:T(8,128)(2,1)} custom-call(f32[4]{0:T(128)} %refs_0_.1, f32[4]{0:T(128)} %refs_1_.1, f32[1,128]{1,0:T(1,128)} %bitcast.9, f32[1,256]{1,0:T(1,128)} %bitcast.6, f32[1,2048]{1,0:T(1,128)} %bitcast.5, s32[2,128]{1,0:T(2,128)} %bitcast.7, f32[2,128]{1,0:T(2,128)} %bitcast.8, bf16[128,4,128]{2,1,0:T(4,128)(2,1)} %refs_7_.1, ...), custom_call_target="tpu_custom_call" | custom-call | tf_op jit(solution)/shard_map/layer/pallas_call | solution.py:907
  87.9 1.6 %copy.21 = bf16[128,512]{1,0:T(8,128)(2,1)} copy(bf16[128,512]{1,0:T(8,128)(2,1)} %layer.1) | data formatting | bytes 262144
